TPU v7x, 32 devices: a whole 2x2x4 slice. The times are simulated.
32 devices in a mesh: ep: 8 (over z, x), tp: 4 (over y, core).
Axes of the slice: x: 2, y: 2, z: 4, core: 2. Of those that a mesh axis runs over, the one named last changes fastest.
Arguments:
- tokens: bfloat16 [4096, 4096], P('ep', 'tp'), may hold values from -100 to 100, as said below
- routes: int32 [4096, 2], P('ep'), may hold values from 0 to 15, all different within a row; in each aligned block of 512 rows (0 to 511, 512 to 1023, ...) at most 128 rows name the same one
- route_weights: float32 [4096, 2], P('ep'), may hold values from 0.1 to 1
- norm_gain: float32 [4096], P('tp'), may hold values from 0.1 to 1.9
- gate_weight: bfloat16 [16, 4096, 512], P('ep', 'tp'), may hold values from -0.09375 to 0.09375
- up_weight: bfloat16 [16, 4096, 512], P('ep', 'tp'), may hold values from -0.09375 to 0.09375
- down_weight: bfloat16 [16, 512, 4096], P('ep', None, 'tp'), may hold values from -0.25 to 0.25
- final_gain: float32 [4096], P('tp'), may hold values from 0.1 to 1.9
Outputs:
- mixed: bfloat16 [4096, 4096], P('ep', 'tp')
Inputs may be any that keep to these rules, and one draw needn't show every extreme that they name: `tokens`: real-valued activations whose features differ in scale. `routes`: each row names 2 different experts; among the 512 rows of one aligned block no expert is named more than 128 times, a bound that some block reaches.
All inputs are finite; a program needn't handle non-finite values.
Results may differ from a plain program's by a relative error of at most 0.018.
Values may be sent and summed in bfloat16 or wider, within the bound.
A program may use at most 64 MiB of HBM per device.

v0:
```python
import functools

import jax
import jax.numpy as jnp
from jax import lax
from jax.experimental import pallas as pl
from jax.experimental.pallas import tpu as pltpu
from jax.sharding import PartitionSpec as P

EPSILON = 1e-06
BF = jnp.bfloat16
F32 = jnp.float32


def dot(a, b):
    return jnp.dot(a, b, preferred_element_type=F32)


def dot_t(a, b):
    return lax.dot_general(a, b, (((0,), (0,)), ((), ())), preferred_element_type=F32)


def kernel(
    n, nt, local, cap, ring, full,
    x_ref, meta_ref, gain_ref, last_gain_ref, gate_hbm, up_hbm, down_hbm, out_ref,
    gate_v, up_v, down_v, xn, acc, tri, rank_t, wt_t, sq, sq2,
    send_x, recv_x, pk_s, pk_r, far_r, meta_r,
    part, recv_p, hid, out_s, out_r,
    w_sem, xs_sem, xr_sem, ks_sem, kr_sem, fs_sem, fr_sem, ms_sem, mr_sem,
    ps_sem, pr_sem, hs_sem, hr_sem, os_sem, or_sem, qs_sem, qr_sem,
):
    me = lax.axis_index("ep")
    my_tp = lax.axis_index("tp")
    ff = gate_v.shape[2]
    fq = ff // nt
    rows_all = x_ref.shape[0]
    half = n // 2
    chunk = rows_all // 2
    count = local * cap
    split = local // 2

    loads = [
        pltpu.make_async_copy(src, dst, w_sem.at[i])
        for i, (src, dst) in enumerate(((gate_hbm, gate_v), (up_hbm, up_v), (down_hbm, down_v)))
    ]
    for load in loads:
        load.start()

    barrier = pltpu.get_barrier_semaphore()

    @pl.loop(1, n)
    def _(s):
        pl.semaphore_signal(barrier, inc=1, device_id={"ep": lax.rem(me + s, n), "tp": my_tp})

    for o in range(1, nt):
        pl.semaphore_signal(barrier, inc=1, device_id={"ep": me, "tp": lax.rem(my_tp + o, nt)})

    place = jnp.where(me % 2 == 0, me // 2, n - 1 - me // 2)

    def at_place(p):
        p = lax.rem(p + 2 * n, n)
        return jnp.where(p < half, 2 * p, 2 * (n - 1 - p) + 1)

    def shift(s):
        return (1 - 2 * ((s + 1) % 2)) * ((s + 1) // 2)

    def source(s):
        if ring:
            return at_place(place - shift(s))
        return lax.rem(me - s + n, n)

    def sender(s):
        if ring:
            return at_place(place + shift(s))
        return lax.rem(me + s, n)

    def eye():
        shape = (rows_all, rows_all)
        return lax.broadcasted_iota(jnp.int32, shape, 0) == lax.broadcasted_iota(jnp.int32, shape, 1)

    def sq_copy(k, o):
        q = lax.rem(my_tp + o, nt)
        return pltpu.make_async_remote_copy(
            sq.at[k], sq2.at[k, o - 1], qs_sem.at[k, o - 1], qr_sem.at[k, o - 1],
            device_id={"ep": me, "tp": q},
        )

    def start_sum(k, column):
        row = jnp.sum(jnp.where(eye(), column, 0.0), axis=0, keepdims=True)
        sq[k] = jnp.broadcast_to(row, sq.shape[1:])

    def send_sum(k):
        for o in range(1, nt):
            sq_copy(k, o).start()

    def finish_sum(k):
        for o in range(1, nt):
            sq_copy(k, o).wait_recv()
        total = sq[k]
        for o in range(1, nt):
            total = total + sq2[k, o - 1]
        scale = lax.rsqrt(total[0:1] / full + EPSILON)
        return jnp.sum(jnp.where(eye(), scale, 0.0), axis=1, keepdims=True)

    def make_table(slot, meta):
        names = lax.broadcasted_iota(jnp.int32, rank_t.shape[1:], 0).astype(F32)
        first, second = meta[0:1] == names, meta[1:2] == names
        hit = first | second
        before = dot(jnp.where(hit, 1.0, 0.0).astype(BF), tri[...])
        rank_t[slot] = jnp.where(hit, before, -1.0)
        wt_t[slot] = jnp.where(first, meta[2:3], 0.0) + jnp.where(second, meta[3:4], 0.0)

    def onehot(slot, expert, weighted=False):
        rank = rank_t[slot, pl.ds(expert, 1), :]
        hit = lax.broadcasted_iota(jnp.int32, (cap, rows_all), 0).astype(F32) == rank
        return jnp.where(hit, wt_t[slot, pl.ds(expert, 1), :] if weighted else F32(1.0), F32(0.0))

    def pack(slot, experts, block):
        pick = jnp.concatenate([onehot(slot, e) for e in experts], axis=0).astype(BF)
        return dot(pick, block).astype(BF)

    def experts_of(owner):
        return [owner * local + j for j in range(local)]

    def x_copy(s):
        return pltpu.make_async_remote_copy(
            send_x.at[s], recv_x.at[s], xs_sem.at[s], xr_sem.at[s],
            device_id={"ep": sender(s), "tp": my_tp},
        )

    def ahead(i):
        return {"ep": at_place(place + 1 - 2 * i), "tp": my_tp}

    def block_copy(d, i, k):
        piece = pl.ds(k * chunk, chunk)
        src = xn.at[piece] if d == 1 else recv_x.at[2 * d - 4 + i, piece]
        slot = 2 * d - 2 + i
        return pltpu.make_async_remote_copy(
            src, recv_x.at[slot, piece], xs_sem.at[slot, k], xr_sem.at[slot, k], device_id=ahead(i)
        )

    def meta_copy(d, i):
        slot = 2 * d - 2 + i
        return pltpu.make_async_remote_copy(
            meta_ref if d == 1 else meta_r.at[slot - 2], meta_r.at[slot],
            ms_sem.at[slot], mr_sem.at[slot], device_id=ahead(i),
        )

    def pack_copy(i):
        return pltpu.make_async_remote_copy(
            pk_s.at[i], pk_r.at[i], ks_sem.at[i], kr_sem.at[i], device_id=ahead(i)
        )

    def far_copy(i):
        return pltpu.make_async_remote_copy(
            pk_r.at[i, pl.ds(count, split * cap)], far_r.at[i], fs_sem.at[i], fr_sem.at[i],
            device_id=ahead(i),
        )

    def p_copy(s, o):
        q = lax.rem(my_tp + o, nt)
        return pltpu.make_async_remote_copy(
            part.at[s, q], recv_p.at[s, o - 1], ps_sem.at[s, o - 1], pr_sem.at[s, o - 1],
            device_id={"ep": me, "tp": q},
        )

    def h_copy(s, o, back=False):
        mine = lax.rem(my_tp - o + nt, nt) if back else my_tp
        q = lax.rem(my_tp - o + nt, nt) if back else lax.rem(my_tp + o, nt)
        return pltpu.make_async_remote_copy(
            hid.at[s, mine], hid.at[s, mine], hs_sem.at[s, o - 1], hr_sem.at[s, o - 1],
            device_id={"ep": me, "tp": q},
        )

    def o_copy(s):
        return pltpu.make_async_remote_copy(
            out_s.at[s], out_r.at[s], os_sem.at[s], or_sem.at[s],
            device_id={"ep": source(s), "tp": my_tp},
        )

    def stage_a(s, rows_of):
        for j in range(local):
            rows = rows_of(j)
            gate = dot(rows, gate_v[j]).astype(BF)
            upper = dot(rows, up_v[j]).astype(BF)
            for q in range(nt):
                part[s, q, pl.ds(j * cap, cap), pl.ds(0, fq)] = gate[:, q * fq:(q + 1) * fq]
                part[s, q, pl.ds(j * cap, cap), pl.ds(fq, fq)] = upper[:, q * fq:(q + 1) * fq]
        for o in range(1, nt):
            p_copy(s, o).start()

    def stage_b(s):
        for o in range(1, nt):
            p_copy(s, o).wait_recv()
        total = part[s, my_tp].astype(F32)
        for o in range(1, nt):
            total = total + recv_p[s, o - 1].astype(F32)
        gate, upper = total[:, :fq], total[:, fq:]
        hid[s, my_tp] = (gate / (1.0 + jnp.exp(-gate)) * upper).astype(BF)
        for o in range(1, nt):
            h_copy(s, o).start()

    def stage_c(s, own):
        for o in range(1, nt):
            h_copy(s, o, True).wait_recv()
        target = out_r if own else out_s
        for j in range(local):
            hidden = jnp.concatenate([hid[s, q, pl.ds(j * cap, cap), :] for q in range(nt)], axis=1)
            target[s, pl.ds(j * cap, cap), :] = dot(hidden, down_v[j]).astype(BF)
        if not own:
            o_copy(s).start()

    def combine(s):
        weight = jnp.concatenate([onehot(0, e, True) for e in experts_of(sender(s))], axis=0)
        high = weight.astype(BF)
        low = (weight - high.astype(F32)).astype(BF)
        rows = out_r[s]
        return dot_t(high, rows) + dot_t(low, rows)

    values = x_ref[...].astype(F32)
    start_sum(0, jnp.sum(values * values, axis=1, keepdims=True))
    shape = (rows_all, rows_all)
    earlier = lax.broadcasted_iota(jnp.int32, shape, 0) < lax.broadcasted_iota(jnp.int32, shape, 1)
    tri[...] = jnp.where(earlier, 1.0, 0.0).astype(BF)
    pl.semaphore_wait(barrier, n - 1 + nt - 1)
    send_sum(0)
    if ring:
        for i in range(2):
            meta_copy(1, i).start()
    make_table(0, meta_ref[...])
    scale = finish_sum(0)
    xn[...] = (x_ref[...].astype(F32) * scale * gain_ref[...]).astype(BF)

    def own_rows(j):
        return pack(0, [me * local + j], xn[...])

    def stored(ref, slot):
        return lambda j: ref[slot, pl.ds(j * cap, cap), :]

    if ring:
        for k in range(2):
            for i in range(2):
                block_copy(1, i, k).start()
        for load in loads:
            load.wait()
        stage_a(0, own_rows)
        for d in range(1, half + 1):
            if d <= half - 2:
                for k in range(2):
                    for i in range(2):
                        block_copy(d, i, k).wait_recv()
                        if d < half - 2:
                            block_copy(d + 1, i, k).start()
                for i in range(2):
                    slot = 2 * d - 2 + i
                    meta_copy(d, i).wait_recv()
                    if d < half - 2:
                        meta_copy(d + 1, i).start()
                    make_table(1 + slot, meta_r[slot])
                if d == half - 2:
                    for i in range(2):
                        slot = 2 * d - 2 + i
                        step = 1 - 2 * i
                        far = experts_of(at_place(place + 2 * step))
                        wanted = experts_of(at_place(place + step)) + (far[split:] if i else far[:split])
                        pk_s[i] = pack(1 + slot, wanted, recv_x[slot])
                        pack_copy(i).start()
            elif d == half - 1:
                for i in range(2):
                    pack_copy(i).wait_recv()
                    far_copy(i).start()
            else:
                for i in range(2):
                    far_copy(i).wait_recv()
            for i in range(2 if d < half else 1):
                s = 2 * d - 1 + i
                slot = s - 1
                if d <= half - 2:
                    stage_a(s, lambda j, slot=slot: pack(1 + slot, [me * local + j], recv_x[slot]))
                elif d == half - 1:
                    stage_a(s, stored(pk_r, i))
                else:
                    stage_a(s, lambda j: far_r[j // split, pl.ds(j % split * cap, cap), :])
                stage_b(s - 1)
                if s >= 2:
                    stage_c(s - 2, s == 2)
    else:
        send_x[1] = pack(0, experts_of(sender(1)), xn[...])

        @pl.loop(2, n)
        def _(s):
            send_x[s] = pack(0, experts_of(sender(s)), xn[...])
            x_copy(s - 1).start()

        for load in loads:
            load.wait()
        stage_a(0, own_rows)
        x_copy(n - 1).start()
        x_copy(1).wait_recv()
        stage_a(1, stored(recv_x, 1))
        stage_b(0)
        x_copy(2).wait_recv()
        stage_a(2, stored(recv_x, 2))
        stage_b(1)
        stage_c(0, True)

        @pl.loop(3, n)
        def _(s):
            x_copy(s).wait_recv()
            stage_a(s, stored(recv_x, s))
            stage_b(s - 1)
            stage_c(s - 2, False)

    stage_b(n - 1)
    stage_c(n - 2, False)
    acc[...] = combine(0)
    stage_c(n - 1, False)

    @pl.loop(1, n)
    def _(s):
        o_copy(s).wait_recv()
        acc[...] += combine(s)

    summed = acc[...]
    start_sum(1, jnp.sum(summed * summed, axis=1, keepdims=True))

    @pl.loop(0, n)
    def _(s):
        for o in range(1, nt):
            p_copy(s, o).wait_send()
            h_copy(s, o).wait_send()

    send_sum(1)

    @pl.loop(1, n)
    def _(s):
        o_copy(s).wait_send()

    if ring:
        for i in range(2):
            for d in range(1, half - 1):
                meta_copy(d, i).wait_send()
                for k in range(2):
                    block_copy(d, i, k).wait_send()
            pack_copy(i).wait_send()
            far_copy(i).wait_send()
    else:
        @pl.loop(1, n)
        def _(s):
            x_copy(s).wait_send()

    scale = finish_sum(1)
    out_ref[...] = (acc[...] * scale * last_gain_ref[...]).astype(BF)
    for k in range(2):
        for o in range(1, nt):
            sq_copy(k, o).wait_send()


RING_BYTES = 24 * 1024 * 1024


def body(tokens, routes, route_weights, norm_gain, gate_weight, up_weight, down_weight, final_gain):
    n, nt = lax.axis_size("ep"), lax.axis_size("tp")
    local, width, ff = gate_weight.shape
    experts = n * local
    rows = tokens.shape[0]
    full = width * nt
    cap = 4 * rows // experts
    count = local * cap
    blocks = max(n - 4, 0)
    ring = n % 2 == 0 and n >= 6 and local % 2 == 0 and blocks * rows * width * 2 <= RING_BYTES
    meta = jnp.concatenate(
        [routes.T.astype(F32), route_weights.T, jnp.zeros((4, rows), F32)], axis=0
    )
    tables = 1 + blocks if ring else 1
    packed = count + local // 2 * cap

    any_spec = pl.BlockSpec(memory_space=pl.ANY)
    vmem = pl.BlockSpec(memory_space=pltpu.VMEM)
    dma = pltpu.SemaphoreType.DMA

    def only(ring_shape, shape, kind=BF):
        return pltpu.VMEM(ring_shape if ring else shape, kind)

    tiny = (1, 16, 128)
    return pl.pallas_call(
        functools.partial(kernel, n, nt, local, cap, ring, full),
        out_shape=jax.ShapeDtypeStruct((rows, width), BF),
        in_specs=[vmem, vmem, vmem, vmem, any_spec, any_spec, any_spec],
        out_specs=vmem,
        scratch_shapes=[
            pltpu.VMEM(gate_weight.shape, BF),
            pltpu.VMEM(up_weight.shape, BF),
            pltpu.VMEM(down_weight.shape, BF),
            pltpu.VMEM((rows, width), BF),
            pltpu.VMEM((rows, width), F32),
            pltpu.VMEM((rows, rows), BF),
            pltpu.VMEM((tables, experts, rows), F32),
            pltpu.VMEM((tables, experts, rows), F32),
            pltpu.VMEM((2, 8, rows), F32),
            pltpu.VMEM((2, nt - 1, 8, rows), F32),
            only(tiny, (n, count, width)),
            only((blocks, rows, width), (n, count, width)),
            only((2, packed, width), tiny),
            only((2, packed, width), tiny),
            only((2, local // 2 * cap, width), tiny),
            only((blocks, 8, rows), (1, 8, 128), F32),
            pltpu.VMEM((n, nt, count, 2 * ff // nt), BF),
            pltpu.VMEM((n, nt - 1, count, 2 * ff // nt), BF),
            pltpu.VMEM((n, nt, count, ff // nt), BF),
            pltpu.VMEM((n, count, width), BF),
            pltpu.VMEM((n, count, width), BF),
            dma((3,)),
            dma((blocks, 2) if ring else (n,)),
            dma((blocks, 2) if ring else (n,)),
            dma((2,)),
            dma((2,)),
            dma((2,)),
            dma((2,)),
            dma((blocks,) if ring else (1,)),
            dma((blocks,) if ring else (1,)),
            dma((n, nt - 1)),
            dma((n, nt - 1)),
            dma((n, nt - 1)),
            dma((n, nt - 1)),
            dma((n,)),
            dma((n,)),
            dma((2, nt - 1)),
            dma((2, nt - 1)),
        ],
        compiler_params=pltpu.CompilerParams(
            collective_id=0, has_side_effects=True, vmem_limit_bytes=60 * 1024 * 1024
        ),
    )(tokens, meta, norm_gain[None], final_gain[None], gate_weight, up_weight, down_weight)


def solution(mesh):
    in_specs = (
        P("ep", "tp"),
        P("ep", None),
        P("ep", None),
        P("tp"),
        P("ep", "tp", None),
        P("ep", "tp", None),
        P("ep", None, "tp"),
        P("tp"),
    )
    return jax.shard_map(body, mesh=mesh, in_specs=in_specs, out_specs=P("ep", "tp"), check_vma=False)
```

profile of v0, /device:TPU:9, one launch (start us, length us, event | category | flops | bytes accessed | tf_op | source)
XLA Modules:
  0.0 181.1 jit_solution(14577639221121656731)
XLA Ops:
  0.0 0.1 pad.2.clone
  0.1 0.7 convert_bitcast_fusion
  0.8 1.4 maximum_maximum_fusion.meta_ref
  2.1 176.7 %shard_map.82 = bf16[512,1024]{1,0:T(8,128)(2,1)} custom-call(bf16[512,1024]{1,0:T(8,128)(2,1)} %x_ref.1, f32[8,512]{1,0:T(8,128)} %maximum_maximum_fusion.meta_ref, f32[1,1024]{1,0:T(1,128)} %bitcast.5, f32[1,1024]{1,0:T(1,128)} %bitcast.6, bf16[2,1024,512]{2,1,0:T(8,128)(2,1)} %gate_hbm.1, bf16[2,1024,512]{2,1,0:T(8,128)(2,1)} %up_hbm.1, ...), custom_call_target="tpu_custom_call" | custom-call | tf_op jit(solution)/shard_map/pallas_call | solution.py:386
  178.9 2.3 %copy.10 = bf16[512,1024]{1,0:T(8,128)(2,1)} copy(bf16[512,1024]{1,0:T(8,128)(2,1)} %shard_map.82) | data formatting | bytes 2097152
  (1 shorter events, 0.0 us)
where the time goes:
time: 182 us; the launch traced here: 181 us
  Pallas kernels  177 us (97%)
  local copies, waits for them, and re-layouts  2.34 us (1%)
  other arithmetic  2.05 us (1%)
    pallas_call x1, Pallas kernels, body(): pl.pallas_call(functools.partial(kernel, n, nt, local, cap, ring, full),...  177 us

commit v1 on v0

--- a/solution.py
+++ b/solution.py
@@ -356,6 +356,485 @@
             sq_copy(k, o).wait_send()
 
 
+def line_kernel(
+    n, nt, local, cap, full, parts,
+    x_ref, meta_ref, gain_ref, last_gain_ref, gate_hbm, up_hbm, down_hbm, out_ref,
+    gate_v, up_v, down_v, xs, notes, scale_s, tri, cols, pick, lift, rows_o, pk_s, pk_r,
+    part, recv_p, hid, out_o, ret_s, ret_r, comb, sum_s, sum_r, acc, sq, sq2,
+    w_sem, own_sem, rel_sem, blk_sem, nown_sem, nrel_sem, note_sem, ks_sem, kr_sem,
+    ps_sem, pr_sem, hs_sem, hr_sem, ts_sem, tr_sem, ss_sem, sr_sem, qs_sem, qr_sem,
+):
+    me = lax.axis_index("ep")
+    my_tp = lax.axis_index("tp")
+    ff = gate_v.shape[2]
+    fq = ff // nt
+    rows_all, width = x_ref.shape
+    cw = width // parts
+    count = local * cap
+    last = n // 2 - 1
+    z, side = me // 2, me % 2
+    low = z <= last // 2
+    inner = (z >= 1) & (z <= last - 1)
+    end = jnp.logical_not(inner)
+    step_in = jnp.where(low, 2, -2)
+    inward = {"ep": me + step_in, "tp": my_tp}
+    outward = {"ep": jnp.where(inner, me - step_in, me + step_in), "tp": my_tp}
+    mate = me + 1 - 2 * side
+    across = {"ep": mate, "tp": my_tp}
+    spare = last + 1
+
+    def block(s):
+        if s == 0:
+            return z
+        near = jnp.where(inner, 0, 1) if s == 1 else (last if s == 2 else last - 1)
+        return jnp.where(low, near, last - near)
+
+    loads = [
+        pltpu.make_async_copy(src, dst, w_sem.at[i])
+        for i, (src, dst) in enumerate(((gate_hbm, gate_v), (up_hbm, up_v), (down_hbm, down_v)))
+    ]
+    for load in loads:
+        load.start()
+
+    barrier = pltpu.get_barrier_semaphore()
+    pl.semaphore_signal(barrier, inc=1, device_id=inward)
+    pl.semaphore_signal(barrier, inc=1, device_id=across)
+
+    @pl.when(inner)
+    def _():
+        pl.semaphore_signal(barrier, inc=1, device_id=outward)
+
+    for o in range(1, nt):
+        pl.semaphore_signal(barrier, inc=1, device_id={"ep": me, "tp": lax.rem(my_tp + o, nt)})
+
+    def col(c):
+        return pl.ds(c * cw, cw)
+
+    def dcol(c):
+        return pl.ds(pl.multiple_of(c * cw, cw), cw)
+
+    def eye():
+        shape = (rows_all, rows_all)
+        return lax.broadcasted_iota(jnp.int32, shape, 0) == lax.broadcasted_iota(jnp.int32, shape, 1)
+
+    def sq_copy(k, o):
+        q = lax.rem(my_tp + o, nt)
+        return pltpu.make_async_remote_copy(
+            sq.at[k], sq2.at[k, o - 1], qs_sem.at[k, o - 1], qr_sem.at[k, o - 1],
+            device_id={"ep": me, "tp": q},
+        )
+
+    def start_sum(k, column):
+        row = jnp.sum(jnp.where(eye(), column, 0.0), axis=0, keepdims=True)
+        sq[k] = jnp.broadcast_to(row, sq.shape[1:])
+
+    def send_sum(k):
+        for o in range(1, nt):
+            sq_copy(k, o).start()
+
+    def finish_sum(k):
+        for o in range(1, nt):
+            sq_copy(k, o).wait_recv()
+        total = sq[k]
+        for o in range(1, nt):
+            total = total + sq2[k, o - 1]
+        return lax.rsqrt(total / full + EPSILON)
+
+    def own_copy(d, c):
+        return pltpu.make_async_remote_copy(
+            x_ref.at[:, col(c)], xs.at[z, :, col(c)], own_sem.at[d, c], blk_sem.at[z, c],
+            device_id=outward if d else inward,
+        )
+
+    def relay(s, c):
+        b = block(s)
+        return pltpu.make_async_remote_copy(
+            xs.at[b, :, col(c)], xs.at[b, :, col(c)], rel_sem.at[s - 1, c], blk_sem.at[b, c],
+            device_id=inward if s == 1 else outward,
+        )
+
+    def own_note(k, d):
+        return pltpu.make_async_remote_copy(
+            scale_s if k else meta_ref, notes.at[k, z], nown_sem.at[k, d], note_sem.at[k, z],
+            device_id=outward if d else inward,
+        )
+
+    def relay_note(k, s):
+        b = block(s)
+        return pltpu.make_async_remote_copy(
+            notes.at[k, b], notes.at[k, b], nrel_sem.at[k, s - 1], note_sem.at[k, b],
+            device_id=inward if s == 1 else outward,
+        )
+
+    def pack_copy(s, c):
+        return pltpu.make_async_remote_copy(
+            pk_s.at[s, :, col(c)], pk_r.at[s, :, col(c)], ks_sem.at[s, c], kr_sem.at[s, c],
+            device_id=across,
+        )
+
+    def ret_copy(s, c, at):
+        return pltpu.make_async_remote_copy(
+            ret_s.at[s, :, at(c)], ret_r.at[s, :, at(c)], ts_sem.at[s, c], tr_sem.at[s, c],
+            device_id=across,
+        )
+
+    def sum_copy(s, c, at):
+        slot = jnp.where(end, spare, block(s)) if s == 1 else block(s)
+        ep = jnp.where(inner, outward["ep"], inward["ep"]) if s == 1 else inward["ep"]
+        return pltpu.make_async_remote_copy(
+            sum_s.at[s - 1, :, at(c)], sum_r.at[slot, :, at(c)], ss_sem.at[s - 1, c], sr_sem.at[slot, c],
+            device_id={"ep": ep, "tp": my_tp},
+        )
+
+    def sum_wait(slot, c, at):
+        pltpu.make_async_remote_copy(
+            sum_s.at[0, :, at(c)], sum_r.at[slot, :, at(c)], ss_sem.at[0, c], sr_sem.at[slot, c],
+            device_id=inward,
+        ).wait_recv()
+
+    def p_copy(i, o):
+        q = lax.rem(my_tp + o, nt)
+        return pltpu.make_async_remote_copy(
+            part.at[i, q], recv_p.at[i, o - 1], ps_sem.at[i, o - 1], pr_sem.at[i, o - 1],
+            device_id={"ep": me, "tp": q},
+        )
+
+    def h_copy(i, o, back=False):
+        mine = lax.rem(my_tp - o + nt, nt) if back else my_tp
+        q = lax.rem(my_tp - o + nt, nt) if back else lax.rem(my_tp + o, nt)
+        return pltpu.make_async_remote_copy(
+            hid.at[i, mine], hid.at[i, mine], hs_sem.at[i, o - 1], hr_sem.at[i, o - 1],
+            device_id={"ep": me, "tp": q},
+        )
+
+    def prepare(s, meta, scale):
+        row = lax.broadcasted_iota(jnp.int32, (16, rows_all), 0)
+        name = jnp.where(row < local, me * local + row, mate * local + row - local)
+        name = jnp.where(row < 2 * local, name, -1).astype(F32)
+        first, second = meta[0:1] == name, meta[1:2] == name
+        hit = first | second
+        before = dot(jnp.where(hit, 1.0, 0.0).astype(BF), tri[...])
+        rank = jnp.where(hit, before, -1.0)
+        weight = jnp.where(first, meta[2:3], 0.0) + jnp.where(second, meta[3:4], 0.0)
+        blank = jnp.zeros((128 - 32, rows_all), F32)
+        cols[s] = jnp.concatenate([rank, weight, blank], axis=0).T
+        spot = lax.broadcasted_iota(jnp.int32, (cap, rows_all), 0).astype(F32)
+        for e in range(2 * local):
+            at = pl.ds(e * cap, cap)
+            here = spot == rank[e:e + 1]
+            pick[at, :] = jnp.where(here, 1.0, 0.0).astype(BF)
+            total = jnp.sum(jnp.where(here, scale[0:1], 0.0), axis=1, keepdims=True)
+            lift[at, :] = jnp.broadcast_to(total, (cap, lift.shape[1]))
+
+    def pack(s, c):
+        values = x_ref[:, col(c)] if s == 0 else xs[block(s), :, col(c)]
+        gain = gain_ref[:, col(c)]
+        far = dot(pick[pl.ds(count, count), :], values) * lift[pl.ds(count, count), 0:1] * gain
+        pk_s[s, :, col(c)] = far.astype(BF)
+        pack_copy(s, c).start()
+        near = dot(pick[pl.ds(0, count), :], values) * lift[pl.ds(0, count), 0:1] * gain
+        rows_o[:, col(c)] = near.astype(BF)
+
+    def stage_a(s, h):
+        i = 2 * s + h
+        if h:
+            for c in range(parts):
+                pack_copy(s, c).wait_recv()
+        for j in range(local):
+            at = pl.ds(j * cap, cap)
+            rows = pk_r[s, at, :] if h else rows_o[at, :]
+            gate = dot(rows, gate_v[j]).astype(BF)
+            upper = dot(rows, up_v[j]).astype(BF)
+            for q in range(nt):
+                part[i, q, at, pl.ds(0, fq)] = gate[:, q * fq:(q + 1) * fq]
+                part[i, q, at, pl.ds(fq, fq)] = upper[:, q * fq:(q + 1) * fq]
+        for o in range(1, nt):
+            p_copy(i, o).start()
+
+    def stage_b(s, h):
+        i = 2 * s + h
+        for o in range(1, nt):
+            p_copy(i, o).wait_recv()
+        total = part[i, my_tp].astype(F32)
+        for o in range(1, nt):
+            total = total + recv_p[i, o - 1].astype(F32)
+        gate, upper = total[:, :fq], total[:, fq:]
+        hid[i, my_tp] = (gate / (1.0 + jnp.exp(-gate)) * upper).astype(BF)
+        for o in range(1, nt):
+            h_copy(i, o).start()
+
+    def stage_c(s, h):
+        i = 2 * s + h
+        for o in range(1, nt):
+            h_copy(i, o, True).wait_recv()
+        hidden = [
+            jnp.concatenate([hid[i, q, pl.ds(j * cap, cap), :] for q in range(nt)], axis=1)
+            for j in range(local)
+        ]
+        for c in range(parts if h else 1):
+            piece = col(c) if h else pl.ds(0, width)
+            target = ret_s if h else out_o
+            for j in range(local):
+                target[s, pl.ds(j * cap, cap), piece] = dot(hidden[j], down_v[j, :, piece]).astype(BF)
+            if h:
+                ret_copy(s, c, col).start()
+
+    def weave(s):
+        table = cols[s]
+        spot = lax.broadcasted_iota(jnp.int32, (rows_all, cap), 1).astype(F32)
+        for e in range(2 * local):
+            here = spot == table[:, e:e + 1]
+            comb[:, pl.ds(e * cap, cap)] = jnp.where(here, table[:, 16 + e:17 + e], 0.0).astype(BF)
+
+    def mix(s, c):
+        ret_copy(s, c, dcol).wait_recv()
+        near = dot(comb[:, pl.ds(0, count)], out_o[s, :, dcol(c)])
+        return near + dot(comb[:, pl.ds(count, count)], ret_r[s, :, dcol(c)])
+
+    def stage_d(s, more):
+        weave(s)
+
+        @pl.loop(0, parts)
+        def _(c):
+            total = mix(s, c)
+            if more:
+                sum_wait(block(s), c, dcol)
+                total = total + sum_r[block(s), :, dcol(c)].astype(F32)
+            sum_s[s - 1, :, dcol(c)] = total.astype(BF)
+            sum_copy(s, c, dcol).start()
+
+    def heads(lead):
+        for c in lead:
+            own_copy(0, c).start()
+
+            @pl.when(inner)
+            def _(c=c):
+                own_copy(1, c).start()
+
+    def send_note(k):
+        own_note(k, 0).start()
+
+        @pl.when(inner)
+        def _():
+            own_note(k, 1).start()
+
+    def take_notes(s):
+        for k in range(2):
+            relay_note(k, s).wait_recv()
+
+            @pl.when(inner)
+            def _(k=k):
+                relay_note(k, s).start()
+
+    half = parts // 2
+    ahead = {}
+    for c in range(parts):
+        ahead[(1, c)] = [(1, c)]
+    for c in range(parts):
+        spot = parts - half + c
+        ahead.setdefault((1 + spot // parts, spot % parts), []).append((2, c))
+    for c in range(parts):
+        spot = parts + half - 1 + max(c - half + 1, 0)
+        ahead.setdefault((1 + spot // parts, spot % parts), []).append((3, c))
+
+    def arrive(s, c):
+        @pl.when(inner)
+        def _():
+            for item in ahead.get((s, c), ()):
+                relay(*item).wait_recv()
+                relay(*item).start()
+            if (s, c) == (1, parts - 1):
+                for k in range(half, parts):
+                    own_copy(0, k).start()
+
+        @pl.when(end)
+        def _():
+            relay(s, c).wait_recv()
+
+    pl.semaphore_wait(barrier, jnp.where(inner, 3, 2) + nt - 1)
+    send_note(0)
+    heads(range(half))
+    values = x_ref[...].astype(F32)
+    start_sum(0, jnp.sum(values * values, axis=1, keepdims=True))
+    send_sum(0)
+    shape = (rows_all, rows_all)
+    earlier = lax.broadcasted_iota(jnp.int32, shape, 0) < lax.broadcasted_iota(jnp.int32, shape, 1)
+    tri[...] = jnp.where(earlier, 1.0, 0.0).astype(BF)
+    scale_s[...] = finish_sum(0)
+    send_note(1)
+    for c in range(half, parts):
+        @pl.when(end)
+        def _(c=c):
+            own_copy(0, c).start()
+
+        @pl.when(inner)
+        def _(c=c):
+            own_copy(1, c).start()
+
+    prepare(0, meta_ref[...], scale_s[...])
+    for c in range(parts):
+        pack(0, c)
+    for load in loads:
+        load.wait()
+    stage_a(0, 0)
+
+    for s in range(1, last + 1):
+        take_notes(s)
+        prepare(s, notes[0, block(s)], notes[1, block(s)])
+        for c in range(parts):
+            arrive(s, c)
+            pack(s, c)
+            if c == 0:
+                stage_a(s - 1, 1)
+                stage_b(s - 1, 0)
+            elif c == 1:
+                stage_b(s - 1, 1)
+                stage_c(s - 1, 0)
+            elif c == 2:
+                stage_c(s - 1, 1)
+        stage_a(s, 0)
+        if s >= 2:
+            @pl.when(end)
+            def _(s=s):
+                stage_d(s - 1, False)
+
+    stage_a(last, 1)
+    stage_b(last, 0)
+    stage_b(last, 1)
+    stage_c(last, 0)
+    stage_c(last, 1)
+
+    @pl.when(end)
+    def _():
+        stage_d(last, False)
+
+    @pl.when(inner)
+    def _():
+        stage_d(2, True)
+        stage_d(1, True)
+        stage_d(3, True)
+
+    weave(0)
+
+    @pl.loop(0, parts)
+    def _(c):
+        acc[:, dcol(c)] = mix(0, c)
+
+    @pl.when(inner)
+    def _():
+        @pl.loop(0, parts)
+        def _(c):
+            sum_wait(spare, c, dcol)
+            acc[:, dcol(c)] += sum_r[spare, :, dcol(c)].astype(F32)
+
+    @pl.loop(0, parts)
+    def _(c):
+        sum_wait(z, c, dcol)
+        acc[:, dcol(c)] += sum_r[z, :, dcol(c)].astype(F32)
+
+    summed = acc[...]
+    start_sum(1, jnp.sum(summed * summed, axis=1, keepdims=True))
+    send_sum(1)
+
+    for i in range(2 * last + 2):
+        for o in range(1, nt):
+            p_copy(i, o).wait_send()
+            h_copy(i, o).wait_send()
+    for s in range(last + 1):
+        for c in range(parts):
+            pack_copy(s, c).wait_send()
+            ret_copy(s, c, col).wait_send()
+            if s:
+                sum_copy(s, c, col).wait_send()
+    for c in range(parts):
+        own_copy(0, c).wait_send()
+    for k in range(2):
+        own_note(k, 0).wait_send()
+
+    @pl.when(inner)
+    def _():
+        for c in range(parts):
+            own_copy(1, c).wait_send()
+            for s in range(1, last + 1):
+                relay(s, c).wait_send()
+        for k in range(2):
+            own_note(k, 1).wait_send()
+            for s in range(1, last + 1):
+                relay_note(k, s).wait_send()
+
+    scale = jnp.sum(jnp.where(eye(), finish_sum(1)[0:1], 0.0), axis=1, keepdims=True)
+    out_ref[...] = (acc[...] * scale * last_gain_ref[...]).astype(BF)
+    for k in range(2):
+        for o in range(1, nt):
+            sq_copy(k, o).wait_send()
+
+
+def line_call(n, nt, local, cap, full, tokens, meta, norm_gain, gate_weight, up_weight, down_weight, final_gain):
+    rows, width = tokens.shape
+    ff = gate_weight.shape[2]
+    line = n // 2
+    count = local * cap
+    parts = 4
+    any_spec = pl.BlockSpec(memory_space=pl.ANY)
+    vmem = pl.BlockSpec(memory_space=pltpu.VMEM)
+    dma = pltpu.SemaphoreType.DMA
+    return pl.pallas_call(
+        functools.partial(line_kernel, n, nt, local, cap, full, parts),
+        out_shape=jax.ShapeDtypeStruct((rows, width), BF),
+        in_specs=[vmem, vmem, vmem, vmem, any_spec, any_spec, any_spec],
+        out_specs=vmem,
+        scratch_shapes=[
+            pltpu.VMEM(gate_weight.shape, BF),
+            pltpu.VMEM(up_weight.shape, BF),
+            pltpu.VMEM(down_weight.shape, BF),
+            pltpu.VMEM((line, rows, width), BF),
+            pltpu.VMEM((2, line, 8, rows), F32),
+            pltpu.VMEM((8, rows), F32),
+            pltpu.VMEM((rows, rows), BF),
+            pltpu.VMEM((line, rows, 128), F32),
+            pltpu.VMEM((2 * count, rows), BF),
+            pltpu.VMEM((2 * count, 128), F32),
+            pltpu.VMEM((count, width), BF),
+            pltpu.VMEM((line, count, width), BF),
+            pltpu.VMEM((line, count, width), BF),
+            pltpu.VMEM((n, nt, count, 2 * ff // nt), BF),
+            pltpu.VMEM((n, nt - 1, count, 2 * ff // nt), BF),
+            pltpu.VMEM((n, nt, count, ff // nt), BF),
+            pltpu.VMEM((line, count, width), BF),
+            pltpu.VMEM((line, count, width), BF),
+            pltpu.VMEM((line, count, width), BF),
+            pltpu.VMEM((rows, 2 * count), BF),
+            pltpu.VMEM((line - 1, rows, width), BF),
+            pltpu.VMEM((line + 1, rows, width), BF),
+            pltpu.VMEM((rows, width), F32),
+            pltpu.VMEM((2, 8, rows), F32),
+            pltpu.VMEM((2, nt - 1, 8, rows), F32),
+            dma((3,)),
+            dma((2, parts)),
+            dma((line - 1, parts)),
+            dma((line, parts)),
+            dma((2, 2)),
+            dma((2, line - 1)),
+            dma((2, line)),
+            dma((line, parts)),
+            dma((line, parts)),
+            dma((n, nt - 1)),
+            dma((n, nt - 1)),
+            dma((n, nt - 1)),
+            dma((n, nt - 1)),
+            dma((line, parts)),
+            dma((line, parts)),
+            dma((line - 1, parts)),
+            dma((line + 1, parts)),
+            dma((2, nt - 1)),
+            dma((2, nt - 1)),
+        ],
+        compiler_params=pltpu.CompilerParams(
+            collective_id=0, has_side_effects=True, vmem_limit_bytes=62 * 1024 * 1024
+        ),
+    )(tokens, meta, norm_gain[None], final_gain[None], gate_weight, up_weight, down_weight)
+
+
 RING_BYTES = 24 * 1024 * 1024
 
 
@@ -372,6 +851,10 @@
     meta = jnp.concatenate(
         [routes.T.astype(F32), route_weights.T, jnp.zeros((4, rows), F32)], axis=0
     )
+    if n == 8 and local <= 8 and width % 512 == 0 and cap % 128 == 0:
+        return line_call(
+            n, nt, local, cap, full, tokens, meta, norm_gain, gate_weight, up_weight, down_weight, final_gain
+        )
     tables = 1 + blocks if ring else 1
     packed = count + local // 2 * cap
 

time: 182 us -> 187 us (1.027)
  Pallas kernels: 177 us -> 182 us
    pallas_call x1, Pallas kernels: 177 us -> 182 us  [line_call(): pl.pallas_call(functools.partial(line_kernel, n, nt, local, cap, full, pa...]
where the time goes in v1:
time: 187 us; the launch traced here: 186 us
  Pallas kernels  182 us (97%)
  local copies, waits for them, and re-layouts  2.34 us (1%)
  other arithmetic  2.05 us (1%)
    pallas_call x1, Pallas kernels, line_call(): pl.pallas_call(functools.partial(line_kernel, n, nt, local, cap, full, pa...  182 us

profile of v1, /device:TPU:9, one launch (start us, length us, event | category | flops | bytes accessed | tf_op | source)
XLA Modules:
  0.0 186.2 jit_solution(16237917752051348961)
XLA Ops:
  0.0 0.1 pad.2.clone
  0.1 0.7 convert_bitcast_fusion
  0.8 1.4 maximum_maximum_fusion.meta_ref
  2.1 181.8 %shard_map.82 = bf16[512,1024]{1,0:T(8,128)(2,1)} custom-call(bf16[512,1024]{1,0:T(8,128)(2,1)} %x_ref.1, f32[8,512]{1,0:T(8,128)} %maximum_maximum_fusion.meta_ref, f32[1,1024]{1,0:T(1,128)} %bitcast.5, f32[1,1024]{1,0:T(1,128)} %bitcast.6, bf16[2,1024,512]{2,1,0:T(8,128)(2,1)} %gate_hbm.1, bf16[2,1024,512]{2,1,0:T(8,128)(2,1)} %up_hbm.1, ...), custom_call_target="tpu_custom_call" | custom-call | tf_op jit(solution)/shard_map/pallas_call | solution.py:781
  183.9 2.3 %copy.10 = bf16[512,1024]{1,0:T(8,128)(2,1)} copy(bf16[512,1024]{1,0:T(8,128)(2,1)} %shard_map.82) | data formatting | bytes 2097152
  (1 shorter events, 0.0 us)

commit v2 on v1

--- a/solution.py
+++ b/solution.py
@@ -356,12 +356,42 @@
             sq_copy(k, o).wait_send()
 
 
+END_ORDER = (
+    ("a", 0, 0), ("weave", 0), ("prep", 1), ("weave", 1), ("b", 0, 0), ("pack", 1, 0), ("a", 0, 1), ("pack",
+    1, 1), ("c", 0), ("pack", 1, 2), ("pack", 1, 3), ("a", 1, 0), ("prep", 2), ("weave", 2), ("pack", 2, 0),
+    ("a", 1, 1), ("pack", 2, 1), ("b", 1, 0), ("b", 0, 1), ("pack", 2, 2), ("c", 1), ("b", 1, 1), ("c1", 0,
+    0), ("pack", 2, 3), ("a", 2, 0), ("prep", 3), ("weave", 3), ("mix0", 0), ("c1", 1, 0), ("pack", 3, 0),
+    ("a", 2, 1), ("d", 1, 0), ("c1", 1, 1), ("pack", 3, 1), ("b", 2, 0), ("d", 1, 1), ("c1", 1, 2), ("b", 2,
+    1), ("pack", 3, 2), ("c", 2), ("d", 1, 2), ("c1", 1, 3), ("pack", 3, 3), ("a", 3, 0), ("d", 1, 3), ("c1",
+    2, 0), ("c1", 2, 1), ("a", 3, 1), ("d", 2, 0), ("c1", 2, 2), ("d", 2, 1), ("c1", 2, 3), ("b", 3, 0), ("d",
+    2, 2), ("c1", 0, 1), ("b", 3, 1), ("d", 2, 3), ("c1", 0, 2), ("c", 3), ("mix0", 1), ("c1", 0, 3), ("mix0",
+    2), ("c1", 3, 0), ("mix0", 3), ("c1", 3, 1), ("d", 3, 0), ("c1", 3, 2), ("d", 3, 1), ("c1", 3, 3),
+    ("last", 0), ("d", 3, 2), ("d", 3, 3), ("last", 1), ("last", 2), ("last", 3),
+)
+
+INNER_ORDER = (
+    ("a", 0, 0), ("passn", 1), ("passn", 3), ("pass", 1, 0), ("prep", 1), ("weave", 1), ("weave", 0), ("pass",
+    1, 1), ("passn", 2), ("b", 0, 0), ("pack", 1, 0), ("a", 0, 1), ("pack", 1, 1), ("pass", 1, 2), ("pass", 2,
+    0), ("c", 0), ("pack", 1, 2), ("pass", 1, 3), ("pack", 1, 3), ("a", 1, 0), ("prep", 2), ("weave", 2),
+    ("pass", 2, 1), ("ownin", 2), ("ownin", 3), ("pack", 2, 0), ("pack", 2, 1), ("pass", 2, 2), ("b", 0, 1),
+    ("pack", 2, 2), ("b", 1, 0), ("pass", 2, 3), ("pack", 2, 3), ("pass", 3, 0), ("pass", 3, 1), ("a", 1, 1),
+    ("prep", 3), ("weave", 3), ("c1", 0, 0), ("c", 1), ("c1", 0, 1), ("pass", 3, 2), ("a", 2, 1), ("mix0", 0),
+    ("c1", 0, 2), ("mix0", 1), ("c1", 0, 3), ("pass", 3, 3), ("b", 1, 1), ("mix0", 2), ("b", 2, 1), ("mix0",
+    3), ("c1", 1, 0), ("a", 2, 0), ("pack", 3, 0), ("pack", 3, 1), ("pack", 3, 2), ("b", 2, 0), ("spare", 0),
+    ("pack", 3, 3), ("a", 3, 0), ("c", 2), ("c1", 1, 1), ("spare", 1), ("c1", 1, 2), ("a", 3, 1), ("c1", 1,
+    3), ("spare", 2), ("c1", 2, 0), ("b", 3, 0), ("c1", 2, 1), ("b", 3, 1), ("spare", 3), ("c1", 2, 2), ("c",
+    3), ("c1", 2, 3), ("d", 2, 0), ("c1", 3, 0), ("c1", 3, 1), ("d", 2, 1), ("c1", 3, 2), ("d", 1, 0), ("c1",
+    3, 3), ("d", 2, 2), ("d", 1, 1), ("d", 2, 3), ("d", 1, 2), ("d", 3, 0), ("d", 1, 3), ("d", 3, 1), ("last",
+    0), ("d", 3, 2), ("last", 1), ("d", 3, 3), ("last", 2), ("last", 3),
+)
+
+
 def line_kernel(
     n, nt, local, cap, full, parts,
-    x_ref, meta_ref, gain_ref, last_gain_ref, gate_hbm, up_hbm, down_hbm, out_ref,
-    gate_v, up_v, down_v, xs, notes, scale_s, tri, cols, pick, lift, rows_o, pk_s, pk_r,
+    x_hbm, route_ref, weight_ref, gain_ref, last_gain_ref, gate_hbm, up_hbm, down_hbm, out_ref,
+    gate_v, up_v, down_v, x_ref, xs, notes, note_s, tri, cols, pick, lift, pk_s, pk_r,
     part, recv_p, hid, out_o, ret_s, ret_r, comb, sum_s, sum_r, acc, sq, sq2,
-    w_sem, own_sem, rel_sem, blk_sem, nown_sem, nrel_sem, note_sem, ks_sem, kr_sem,
+    w_sem, x_sem, own_sem, rel_sem, blk_sem, nown_sem, nrel_sem, note_sem, ks_sem, kr_sem,
     ps_sem, pr_sem, hs_sem, hr_sem, ts_sem, tr_sem, ss_sem, sr_sem, qs_sem, qr_sem,
 ):
     me = lax.axis_index("ep")
@@ -393,7 +423,11 @@
         pltpu.make_async_copy(src, dst, w_sem.at[i])
         for i, (src, dst) in enumerate(((gate_hbm, gate_v), (up_hbm, up_v), (down_hbm, down_v)))
     ]
-    for load in loads:
+    x_loads = [
+        pltpu.make_async_copy(x_hbm.at[:, pl.ds(c * cw, cw)], x_ref.at[:, pl.ds(c * cw, cw)], x_sem.at[c])
+        for c in range(parts)
+    ]
+    for load in x_loads + loads:
         load.start()
 
     barrier = pltpu.get_barrier_semaphore()
@@ -453,22 +487,21 @@
             device_id=inward if s == 1 else outward,
         )
 
-    def own_note(k, d):
-        return pltpu.make_async_remote_copy(
-            scale_s if k else meta_ref, notes.at[k, z], nown_sem.at[k, d], note_sem.at[k, z],
-            device_id=outward if d else inward,
-        )
-
-    def relay_note(k, s):
+    def own_note(d):
+        return pltpu.make_async_remote_copy(
+            note_s, notes.at[z], nown_sem.at[d], note_sem.at[z], device_id=outward if d else inward
+        )
+
+    def relay_note(s):
         b = block(s)
         return pltpu.make_async_remote_copy(
-            notes.at[k, b], notes.at[k, b], nrel_sem.at[k, s - 1], note_sem.at[k, b],
+            notes.at[b], notes.at[b], nrel_sem.at[s - 1], note_sem.at[b],
             device_id=inward if s == 1 else outward,
         )
 
     def pack_copy(s, c):
         return pltpu.make_async_remote_copy(
-            pk_s.at[s, :, col(c)], pk_r.at[s, :, col(c)], ks_sem.at[s, c], kr_sem.at[s, c],
+            pk_s.at[s, pl.ds(count, count), col(c)], pk_r.at[s, :, col(c)], ks_sem.at[s, c], kr_sem.at[s, c],
             device_id=across,
         )
 
@@ -507,7 +540,8 @@
             device_id={"ep": me, "tp": q},
         )
 
-    def prepare(s, meta, scale):
+    def prepare(s):
+        meta = notes[block(s)] if s else note_s[...]
         row = lax.broadcasted_iota(jnp.int32, (16, rows_all), 0)
         name = jnp.where(row < local, me * local + row, mate * local + row - local)
         name = jnp.where(row < 2 * local, name, -1).astype(F32)
@@ -523,31 +557,37 @@
             at = pl.ds(e * cap, cap)
             here = spot == rank[e:e + 1]
             pick[at, :] = jnp.where(here, 1.0, 0.0).astype(BF)
-            total = jnp.sum(jnp.where(here, scale[0:1], 0.0), axis=1, keepdims=True)
+            total = jnp.sum(jnp.where(here, meta[4:5], 0.0), axis=1, keepdims=True)
             lift[at, :] = jnp.broadcast_to(total, (cap, lift.shape[1]))
 
     def pack(s, c):
-        values = x_ref[:, col(c)] if s == 0 else xs[block(s), :, col(c)]
-        gain = gain_ref[:, col(c)]
-        far = dot(pick[pl.ds(count, count), :], values) * lift[pl.ds(count, count), 0:1] * gain
-        pk_s[s, :, col(c)] = far.astype(BF)
+        values = x_ref.at[:, col(c)] if s == 0 else xs.at[block(s), :, col(c)]
+
+        @pl.loop(0, 2 * local)
+        def _(e):
+            group = pl.ds(pl.multiple_of(e * cap, cap), cap)
+            rows = dot(pick[group, :], values[...]) * lift[group, 0:1] * gain_ref[:, col(c)]
+            pk_s[s, group, col(c)] = rows.astype(BF)
+
         pack_copy(s, c).start()
-        near = dot(pick[pl.ds(0, count), :], values) * lift[pl.ds(0, count), 0:1] * gain
-        rows_o[:, col(c)] = near.astype(BF)
 
     def stage_a(s, h):
         i = 2 * s + h
         if h:
             for c in range(parts):
                 pack_copy(s, c).wait_recv()
-        for j in range(local):
-            at = pl.ds(j * cap, cap)
-            rows = pk_r[s, at, :] if h else rows_o[at, :]
+        source = pk_r if h else pk_s
+
+        @pl.loop(0, local)
+        def _(j):
+            group = pl.ds(pl.multiple_of(j * cap, cap), cap)
+            rows = source[s, group, :]
             gate = dot(rows, gate_v[j]).astype(BF)
             upper = dot(rows, up_v[j]).astype(BF)
             for q in range(nt):
-                part[i, q, at, pl.ds(0, fq)] = gate[:, q * fq:(q + 1) * fq]
-                part[i, q, at, pl.ds(fq, fq)] = upper[:, q * fq:(q + 1) * fq]
+                part[i, q, group, pl.ds(0, fq)] = gate[:, q * fq:(q + 1) * fq]
+                part[i, q, group, pl.ds(fq, fq)] = upper[:, q * fq:(q + 1) * fq]
+
         for o in range(1, nt):
             p_copy(i, o).start()
 
@@ -563,174 +603,151 @@
         for o in range(1, nt):
             h_copy(i, o).start()
 
-    def stage_c(s, h):
-        i = 2 * s + h
-        for o in range(1, nt):
-            h_copy(i, o, True).wait_recv()
-        hidden = [
-            jnp.concatenate([hid[i, q, pl.ds(j * cap, cap), :] for q in range(nt)], axis=1)
-            for j in range(local)
-        ]
-        for c in range(parts if h else 1):
-            piece = col(c) if h else pl.ds(0, width)
-            target = ret_s if h else out_o
-            for j in range(local):
-                target[s, pl.ds(j * cap, cap), piece] = dot(hidden[j], down_v[j, :, piece]).astype(BF)
-            if h:
-                ret_copy(s, c, col).start()
+    def hidden(s, h, j):
+        return jnp.concatenate([hid[2 * s + h, q, pl.ds(j * cap, cap), :] for q in range(nt)], axis=1)
+
+    def take_hidden(s, h):
+        for o in range(1, nt):
+            h_copy(2 * s + h, o, True).wait_recv()
+
+    def stage_c(s):
+        take_hidden(s, 0)
+        for j in range(local):
+            out_o[s, pl.ds(j * cap, cap), :] = dot(hidden(s, 0, j), down_v[j]).astype(BF)
+
+    def send_back(s, c):
+        if c == 0:
+            take_hidden(s, 1)
+        for j in range(local):
+            ret_s[s, pl.ds(j * cap, cap), col(c)] = dot(hidden(s, 1, j), down_v[j, :, col(c)]).astype(BF)
+        ret_copy(s, c, col).start()
 
     def weave(s):
         table = cols[s]
         spot = lax.broadcasted_iota(jnp.int32, (rows_all, cap), 1).astype(F32)
         for e in range(2 * local):
             here = spot == table[:, e:e + 1]
-            comb[:, pl.ds(e * cap, cap)] = jnp.where(here, table[:, 16 + e:17 + e], 0.0).astype(BF)
-
-    def mix(s, c):
-        ret_copy(s, c, dcol).wait_recv()
-        near = dot(comb[:, pl.ds(0, count)], out_o[s, :, dcol(c)])
-        return near + dot(comb[:, pl.ds(count, count)], ret_r[s, :, dcol(c)])
-
-    def stage_d(s, more):
-        weave(s)
-
-        @pl.loop(0, parts)
-        def _(c):
-            total = mix(s, c)
+            comb[s, :, pl.ds(e * cap, cap)] = jnp.where(here, table[:, 16 + e:17 + e], 0.0).astype(BF)
+
+    def mix(s, c, put):
+        ret_copy(s, c, col).wait_recv()
+
+        @pl.loop(0, 2)
+        def _(k):
+            group = pl.ds(pl.multiple_of(k * (rows_all // 2), rows_all // 2), rows_all // 2)
+            near = dot(comb[s, group, pl.ds(0, count)], out_o[s, :, col(c)])
+            put(group, near + dot(comb[s, group, pl.ds(count, count)], ret_r[s, :, col(c)]))
+
+    def stage_d(s, c, more):
+        if more:
+            sum_wait(block(s), c, col)
+
+        def put(group, total):
             if more:
-                sum_wait(block(s), c, dcol)
-                total = total + sum_r[block(s), :, dcol(c)].astype(F32)
-            sum_s[s - 1, :, dcol(c)] = total.astype(BF)
-            sum_copy(s, c, dcol).start()
-
-    def heads(lead):
-        for c in lead:
-            own_copy(0, c).start()
-
-            @pl.when(inner)
-            def _(c=c):
-                own_copy(1, c).start()
-
-    def send_note(k):
-        own_note(k, 0).start()
-
-        @pl.when(inner)
-        def _():
-            own_note(k, 1).start()
-
-    def take_notes(s):
-        for k in range(2):
-            relay_note(k, s).wait_recv()
-
-            @pl.when(inner)
-            def _(k=k):
-                relay_note(k, s).start()
-
-    half = parts // 2
-    ahead = {}
-    for c in range(parts):
-        ahead[(1, c)] = [(1, c)]
-    for c in range(parts):
-        spot = parts - half + c
-        ahead.setdefault((1 + spot // parts, spot % parts), []).append((2, c))
-    for c in range(parts):
-        spot = parts + half - 1 + max(c - half + 1, 0)
-        ahead.setdefault((1 + spot // parts, spot % parts), []).append((3, c))
+                total = total + sum_r[block(s), group, col(c)].astype(F32)
+            sum_s[s - 1, group, col(c)] = total.astype(BF)
+
+        mix(s, c, put)
+        sum_copy(s, c, col).start()
+
+    def own_mix(c):
+        def put(group, total):
+            acc[group, col(c)] = total
+
+        mix(0, c, put)
+
+    def add_spare(c):
+        sum_wait(spare, c, col)
+        acc[:, col(c)] += sum_r[spare, :, col(c)].astype(F32)
+
+    def add_last(c):
+        sum_wait(z, c, col)
+        acc[:, col(c)] += sum_r[z, :, col(c)].astype(F32)
+
+    def pass_on(s, c):
+        relay(s, c).wait_recv()
+        relay(s, c).start()
+
+    def pass_note(s):
+        relay_note(s).wait_recv()
+        relay_note(s).start()
 
     def arrive(s, c):
-        @pl.when(inner)
-        def _():
-            for item in ahead.get((s, c), ()):
-                relay(*item).wait_recv()
-                relay(*item).start()
-            if (s, c) == (1, parts - 1):
-                for k in range(half, parts):
-                    own_copy(0, k).start()
-
-        @pl.when(end)
-        def _():
-            relay(s, c).wait_recv()
+        relay(s, c).wait_recv()
+
+    def take_note(s):
+        relay_note(s).wait_recv()
+
+    def lead(k):
+        own_copy(0, k).start()
+
+    def run(order, at_end):
+        def prep(s):
+            if at_end:
+                take_note(s)
+            prepare(s)
+
+        def bring(s, c):
+            if at_end:
+                arrive(s, c)
+            pack(s, c)
+
+        calls = {
+            "passn": pass_note, "pass": pass_on, "ownin": lead, "prep": prep, "pack": bring,
+            "a": stage_a, "b": stage_b, "c": stage_c, "c1": send_back, "weave": weave, "mix0": own_mix,
+            "d": lambda s, c: stage_d(s, c, not at_end), "spare": add_spare, "last": add_last,
+        }
+        for name, *where in order:
+            calls[name](*where)
 
     pl.semaphore_wait(barrier, jnp.where(inner, 3, 2) + nt - 1)
-    send_note(0)
-    heads(range(half))
+    x_loads[0].wait()
+    own_copy(0, 0).start()
+
+    @pl.when(inner)
+    def _():
+        own_copy(1, 0).start()
+
+    for load in x_loads[1:]:
+        load.wait()
     values = x_ref[...].astype(F32)
     start_sum(0, jnp.sum(values * values, axis=1, keepdims=True))
     send_sum(0)
     shape = (rows_all, rows_all)
     earlier = lax.broadcasted_iota(jnp.int32, shape, 0) < lax.broadcasted_iota(jnp.int32, shape, 1)
     tri[...] = jnp.where(earlier, 1.0, 0.0).astype(BF)
-    scale_s[...] = finish_sum(0)
-    send_note(1)
-    for c in range(half, parts):
-        @pl.when(end)
-        def _(c=c):
+    blank = jnp.zeros((3, rows_all), F32)
+    note_s[...] = jnp.concatenate(
+        [route_ref[...].astype(F32), weight_ref[...], finish_sum(0)[0:1], blank], axis=0
+    )
+    own_note(0).start()
+
+    @pl.when(inner)
+    def _():
+        own_note(1).start()
+        for c in range(1, parts // 2):
             own_copy(0, c).start()
-
-        @pl.when(inner)
-        def _(c=c):
+        for c in range(1, parts):
             own_copy(1, c).start()
 
-    prepare(0, meta_ref[...], scale_s[...])
+    @pl.when(end)
+    def _():
+        for c in range(1, parts):
+            own_copy(0, c).start()
+
+    prepare(0)
     for c in range(parts):
         pack(0, c)
     for load in loads:
         load.wait()
-    stage_a(0, 0)
-
-    for s in range(1, last + 1):
-        take_notes(s)
-        prepare(s, notes[0, block(s)], notes[1, block(s)])
-        for c in range(parts):
-            arrive(s, c)
-            pack(s, c)
-            if c == 0:
-                stage_a(s - 1, 1)
-                stage_b(s - 1, 0)
-            elif c == 1:
-                stage_b(s - 1, 1)
-                stage_c(s - 1, 0)
-            elif c == 2:
-                stage_c(s - 1, 1)
-        stage_a(s, 0)
-        if s >= 2:
-            @pl.when(end)
-            def _(s=s):
-                stage_d(s - 1, False)
-
-    stage_a(last, 1)
-    stage_b(last, 0)
-    stage_b(last, 1)
-    stage_c(last, 0)
-    stage_c(last, 1)
 
     @pl.when(end)
     def _():
-        stage_d(last, False)
+        run(END_ORDER, True)
 
     @pl.when(inner)
     def _():
-        stage_d(2, True)
-        stage_d(1, True)
-        stage_d(3, True)
-
-    weave(0)
-
-    @pl.loop(0, parts)
-    def _(c):
-        acc[:, dcol(c)] = mix(0, c)
-
-    @pl.when(inner)
-    def _():
-        @pl.loop(0, parts)
-        def _(c):
-            sum_wait(spare, c, dcol)
-            acc[:, dcol(c)] += sum_r[spare, :, dcol(c)].astype(F32)
-
-    @pl.loop(0, parts)
-    def _(c):
-        sum_wait(z, c, dcol)
-        acc[:, dcol(c)] += sum_r[z, :, dcol(c)].astype(F32)
+        run(INNER_ORDER, False)
 
     summed = acc[...]
     start_sum(1, jnp.sum(summed * summed, axis=1, keepdims=True))
@@ -748,19 +765,17 @@
                 sum_copy(s, c, col).wait_send()
     for c in range(parts):
         own_copy(0, c).wait_send()
-    for k in range(2):
-        own_note(k, 0).wait_send()
+    own_note(0).wait_send()
 
     @pl.when(inner)
     def _():
+        own_note(1).wait_send()
         for c in range(parts):
             own_copy(1, c).wait_send()
-            for s in range(1, last + 1):
+        for s in range(1, last + 1):
+            relay_note(s).wait_send()
+            for c in range(parts):
                 relay(s, c).wait_send()
-        for k in range(2):
-            own_note(k, 1).wait_send()
-            for s in range(1, last + 1):
-                relay_note(k, s).wait_send()
 
     scale = jnp.sum(jnp.where(eye(), finish_sum(1)[0:1], 0.0), axis=1, keepdims=True)
     out_ref[...] = (acc[...] * scale * last_gain_ref[...]).astype(BF)
@@ -769,7 +784,7 @@
             sq_copy(k, o).wait_send()
 
 
-def line_call(n, nt, local, cap, full, tokens, meta, norm_gain, gate_weight, up_weight, down_weight, final_gain):
+def line_call(n, nt, local, cap, full, tokens, routes, weights, norm_gain, gate_weight, up_weight, down_weight, final_gain):
     rows, width = tokens.shape
     ff = gate_weight.shape[2]
     line = n // 2
@@ -781,21 +796,21 @@
     return pl.pallas_call(
         functools.partial(line_kernel, n, nt, local, cap, full, parts),
         out_shape=jax.ShapeDtypeStruct((rows, width), BF),
-        in_specs=[vmem, vmem, vmem, vmem, any_spec, any_spec, any_spec],
+        in_specs=[any_spec, vmem, vmem, vmem, vmem, any_spec, any_spec, any_spec],
         out_specs=vmem,
         scratch_shapes=[
             pltpu.VMEM(gate_weight.shape, BF),
             pltpu.VMEM(up_weight.shape, BF),
             pltpu.VMEM(down_weight.shape, BF),
+            pltpu.VMEM((rows, width), BF),
             pltpu.VMEM((line, rows, width), BF),
-            pltpu.VMEM((2, line, 8, rows), F32),
+            pltpu.VMEM((line, 8, rows), F32),
             pltpu.VMEM((8, rows), F32),
             pltpu.VMEM((rows, rows), BF),
             pltpu.VMEM((line, rows, 128), F32),
             pltpu.VMEM((2 * count, rows), BF),
             pltpu.VMEM((2 * count, 128), F32),
-            pltpu.VMEM((count, width), BF),
-            pltpu.VMEM((line, count, width), BF),
+            pltpu.VMEM((line, 2 * count, width), BF),
             pltpu.VMEM((line, count, width), BF),
             pltpu.VMEM((n, nt, count, 2 * ff // nt), BF),
             pltpu.VMEM((n, nt - 1, count, 2 * ff // nt), BF),
@@ -803,19 +818,20 @@
             pltpu.VMEM((line, count, width), BF),
             pltpu.VMEM((line, count, width), BF),
             pltpu.VMEM((line, count, width), BF),
-            pltpu.VMEM((rows, 2 * count), BF),
+            pltpu.VMEM((line, rows, 2 * count), BF),
             pltpu.VMEM((line - 1, rows, width), BF),
             pltpu.VMEM((line + 1, rows, width), BF),
             pltpu.VMEM((rows, width), F32),
             pltpu.VMEM((2, 8, rows), F32),
             pltpu.VMEM((2, nt - 1, 8, rows), F32),
             dma((3,)),
+            dma((parts,)),
             dma((2, parts)),
             dma((line - 1, parts)),
             dma((line, parts)),
-            dma((2, 2)),
-            dma((2, line - 1)),
-            dma((2, line)),
+            dma((2,)),
+            dma((line - 1,)),
+            dma((line,)),
             dma((line, parts)),
             dma((line, parts)),
             dma((n, nt - 1)),
@@ -832,7 +848,7 @@
         compiler_params=pltpu.CompilerParams(
             collective_id=0, has_side_effects=True, vmem_limit_bytes=62 * 1024 * 1024
         ),
-    )(tokens, meta, norm_gain[None], final_gain[None], gate_weight, up_weight, down_weight)
+    )(tokens, routes.T, weights.T, norm_gain[None], final_gain[None], gate_weight, up_weight, down_weight)
 
 
 RING_BYTES = 24 * 1024 * 1024
@@ -848,13 +864,13 @@
     count = local * cap
     blocks = max(n - 4, 0)
     ring = n % 2 == 0 and n >= 6 and local % 2 == 0 and blocks * rows * width * 2 <= RING_BYTES
+    if n == 8 and local <= 8 and width % 512 == 0 and cap % 128 == 0:
+        return line_call(
+            n, nt, local, cap, full, tokens, routes, route_weights, norm_gain, gate_weight, up_weight, down_weight, final_gain
+        )
     meta = jnp.concatenate(
         [routes.T.astype(F32), route_weights.T, jnp.zeros((4, rows), F32)], axis=0
     )
-    if n == 8 and local <= 8 and width % 512 == 0 and cap % 128 == 0:
-        return line_call(
-            n, nt, local, cap, full, tokens, meta, norm_gain, gate_weight, up_weight, down_weight, final_gain
-        )
     tables = 1 + blocks if ring else 1
     packed = count + local // 2 * cap
 

time: 187 us -> 147 us (0.79)
  Pallas kernels: 182 us -> 144 us
  other arithmetic: 2.05 us -> 0 us
    pallas_call x1, Pallas kernels: 182 us -> 144 us  [line_call(): pl.pallas_call(functools.partial(line_kernel, n, nt, local, cap, full, pa...]
where the time goes in v2:
time: 147 us; the launch traced here: 146 us
  Pallas kernels  144 us (98%)
  local copies, waits for them, and re-layouts  2.26 us (2%)
    pallas_call x1, Pallas kernels, line_call(): pl.pallas_call(functools.partial(line_kernel, n, nt, local, cap, full, pa...  144 us

profile of v2, /device:TPU:9, one launch (start us, length us, event | category | flops | bytes accessed | tf_op | source)
XLA Modules:
  0.0 146.4 jit_solution(6348567309203759539)
XLA Ops:
  0.0 144.1 %shard_map.82 = bf16[512,1024]{1,0:T(8,128)(2,1)} custom-call(bf16[512,1024]{1,0:T(8,128)(2,1)} %x_hbm.1, s32[2,512]{1,0:T(2,128)} %bitcast.4, f32[2,512]{1,0:T(2,128)} %bitcast.5, f32[1,1024]{1,0:T(1,128)} %bitcast.6, f32[1,1024]{1,0:T(1,128)} %bitcast.7, bf16[2,1024,512]{2,1,0:T(8,128)(2,1)} %gate_hbm.1, bf16[2,1024,512]{2,1,0:T(8,128)(2,1)} %up_hbm.1, ...), custom_call_target="tpu_custom_call" | custom-call | tf_op jit(solution)/shard_map/pallas_call | solution.py:796
  144.1 2.3 %copy.10 = bf16[512,1024]{1,0:T(8,128)(2,1)} copy(bf16[512,1024]{1,0:T(8,128)(2,1)} %shard_map.82) | data formatting | bytes 2097152

commit v3 on v2

--- a/solution.py
+++ b/solution.py
@@ -357,41 +357,41 @@
 
 
 END_ORDER = (
-    ("a", 0, 0), ("weave", 0), ("prep", 1), ("weave", 1), ("b", 0, 0), ("pack", 1, 0), ("a", 0, 1), ("pack",
-    1, 1), ("c", 0), ("pack", 1, 2), ("pack", 1, 3), ("a", 1, 0), ("prep", 2), ("weave", 2), ("pack", 2, 0),
-    ("a", 1, 1), ("pack", 2, 1), ("b", 1, 0), ("b", 0, 1), ("pack", 2, 2), ("c", 1), ("b", 1, 1), ("c1", 0,
-    0), ("pack", 2, 3), ("a", 2, 0), ("prep", 3), ("weave", 3), ("mix0", 0), ("c1", 1, 0), ("pack", 3, 0),
-    ("a", 2, 1), ("d", 1, 0), ("c1", 1, 1), ("pack", 3, 1), ("b", 2, 0), ("d", 1, 1), ("c1", 1, 2), ("b", 2,
-    1), ("pack", 3, 2), ("c", 2), ("d", 1, 2), ("c1", 1, 3), ("pack", 3, 3), ("a", 3, 0), ("d", 1, 3), ("c1",
-    2, 0), ("c1", 2, 1), ("a", 3, 1), ("d", 2, 0), ("c1", 2, 2), ("d", 2, 1), ("c1", 2, 3), ("b", 3, 0), ("d",
-    2, 2), ("c1", 0, 1), ("b", 3, 1), ("d", 2, 3), ("c1", 0, 2), ("c", 3), ("mix0", 1), ("c1", 0, 3), ("mix0",
-    2), ("c1", 3, 0), ("mix0", 3), ("c1", 3, 1), ("d", 3, 0), ("c1", 3, 2), ("d", 3, 1), ("c1", 3, 3),
-    ("last", 0), ("d", 3, 2), ("d", 3, 3), ("last", 1), ("last", 2), ("last", 3),
+    ("prep", 1), ("a", 0, 0), ("pack", 1, 0), ("b", 0, 0), ("pack", 1, 1), ("pack", 1, 2), ("a", 0, 1), ("b",
+    0, 1), ("pack", 1, 3), ("prep", 2), ("a", 1, 0), ("a", 1, 1), ("c1", 0, 0), ("weave", 1), ("pack", 2, 0),
+    ("pack", 2, 1), ("b", 1, 0), ("b", 1, 1), ("pack", 2, 2), ("pack", 2, 3), ("a", 2, 0), ("c1", 1, 0),
+    ("c1", 1, 1), ("c1", 1, 2), ("a", 2, 1), ("c", 1), ("d", 1, 0), ("b", 2, 0), ("prep", 3), ("pack", 3, 0),
+    ("pack", 3, 1), ("weave", 2), ("d", 1, 1), ("b", 2, 1), ("d", 1, 2), ("pack", 3, 2), ("c1", 2, 0),
+    ("pack", 3, 3), ("c1", 2, 1), ("a", 3, 0), ("c", 2), ("d", 2, 0), ("c1", 2, 2), ("c1", 2, 3), ("c1", 0,
+    1), ("a", 3, 1), ("d", 2, 1), ("d", 2, 3), ("b", 3, 1), ("b", 3, 0), ("weave", 0), ("d", 2, 2), ("c1", 1,
+    3), ("weave", 3), ("c", 0), ("c1", 3, 0), ("c1", 3, 1), ("c", 3), ("d", 3, 0), ("mix0", 1), ("c1", 0, 2),
+    ("d", 3, 1), ("c1", 3, 2), ("c1", 3, 3), ("d", 3, 2), ("mix0", 0), ("c1", 0, 3), ("d", 3, 3), ("mix0", 2),
+    ("last", 0), ("mix0", 3), ("last", 3), ("d", 1, 3), ("last", 1), ("last", 2),
 )
 
 INNER_ORDER = (
-    ("a", 0, 0), ("passn", 1), ("passn", 3), ("pass", 1, 0), ("prep", 1), ("weave", 1), ("weave", 0), ("pass",
-    1, 1), ("passn", 2), ("b", 0, 0), ("pack", 1, 0), ("a", 0, 1), ("pack", 1, 1), ("pass", 1, 2), ("pass", 2,
-    0), ("c", 0), ("pack", 1, 2), ("pass", 1, 3), ("pack", 1, 3), ("a", 1, 0), ("prep", 2), ("weave", 2),
-    ("pass", 2, 1), ("ownin", 2), ("ownin", 3), ("pack", 2, 0), ("pack", 2, 1), ("pass", 2, 2), ("b", 0, 1),
-    ("pack", 2, 2), ("b", 1, 0), ("pass", 2, 3), ("pack", 2, 3), ("pass", 3, 0), ("pass", 3, 1), ("a", 1, 1),
-    ("prep", 3), ("weave", 3), ("c1", 0, 0), ("c", 1), ("c1", 0, 1), ("pass", 3, 2), ("a", 2, 1), ("mix0", 0),
-    ("c1", 0, 2), ("mix0", 1), ("c1", 0, 3), ("pass", 3, 3), ("b", 1, 1), ("mix0", 2), ("b", 2, 1), ("mix0",
-    3), ("c1", 1, 0), ("a", 2, 0), ("pack", 3, 0), ("pack", 3, 1), ("pack", 3, 2), ("b", 2, 0), ("spare", 0),
-    ("pack", 3, 3), ("a", 3, 0), ("c", 2), ("c1", 1, 1), ("spare", 1), ("c1", 1, 2), ("a", 3, 1), ("c1", 1,
-    3), ("spare", 2), ("c1", 2, 0), ("b", 3, 0), ("c1", 2, 1), ("b", 3, 1), ("spare", 3), ("c1", 2, 2), ("c",
-    3), ("c1", 2, 3), ("d", 2, 0), ("c1", 3, 0), ("c1", 3, 1), ("d", 2, 1), ("c1", 3, 2), ("d", 1, 0), ("c1",
-    3, 3), ("d", 2, 2), ("d", 1, 1), ("d", 2, 3), ("d", 1, 2), ("d", 3, 0), ("d", 1, 3), ("d", 3, 1), ("last",
-    0), ("d", 3, 2), ("last", 1), ("d", 3, 3), ("last", 2), ("last", 3),
+    ("a", 0, 0), ("passn", 1), ("prep", 1), ("pass", 1, 0), ("b", 0, 0), ("pass", 1, 1), ("pack", 1, 0),
+    ("pack", 1, 1), ("a", 0, 1), ("weave", 0), ("passn", 2), ("pass", 2, 0), ("pass", 1, 2), ("pack", 1, 2),
+    ("pass", 1, 3), ("c", 0), ("pack", 1, 3), ("prep", 2), ("pass", 2, 1), ("pass", 2, 2), ("a", 1, 0),
+    ("pass", 2, 3), ("ownin", 2), ("ownin", 3), ("pack", 2, 0), ("b", 0, 1), ("pack", 2, 1), ("pack", 2, 2),
+    ("a", 1, 1), ("pack", 2, 3), ("passn", 3), ("weave", 1), ("c1", 0, 0), ("prep", 3), ("pass", 3, 0), ("a",
+    2, 0), ("pass", 3, 1), ("pack", 3, 0), ("b", 1, 0), ("pass", 3, 2), ("pass", 3, 3), ("a", 2, 1), ("pack",
+    3, 1), ("pack", 3, 2), ("b", 1, 1), ("b", 2, 1), ("pack", 3, 3), ("a", 3, 0), ("c1", 0, 1), ("mix0", 1),
+    ("mix0", 0), ("c1", 2, 0), ("b", 2, 0), ("c1", 2, 1), ("c1", 2, 2), ("c1", 2, 3), ("weave", 2), ("b", 3,
+    0), ("weave", 3), ("a", 3, 1), ("c1", 1, 0), ("c", 2), ("d", 2, 0), ("b", 3, 1), ("d", 2, 1), ("c1", 1,
+    1), ("c1", 1, 2), ("c1", 1, 3), ("c", 3), ("c", 1), ("d", 1, 0), ("c1", 3, 0), ("d", 2, 3), ("d", 1, 1),
+    ("d", 2, 2), ("c1", 3, 1), ("c1", 3, 2), ("c1", 3, 3), ("c1", 0, 2), ("c1", 0, 3), ("d", 1, 3), ("d", 3,
+    0), ("d", 1, 2), ("d", 3, 1), ("d", 3, 2), ("mix0", 3), ("spare", 1), ("d", 3, 3), ("last", 1), ("spare",
+    0), ("last", 0), ("mix0", 2), ("spare", 2), ("spare", 3), ("last", 2), ("last", 3),
 )
 
 
 def line_kernel(
     n, nt, local, cap, full, parts,
-    x_hbm, route_ref, weight_ref, gain_ref, last_gain_ref, gate_hbm, up_hbm, down_hbm, out_ref,
-    gate_v, up_v, down_v, x_ref, xs, notes, note_s, tri, cols, pick, lift, pk_s, pk_r,
+    x_hbm, route_hbm, weight_hbm, gain_hbm, last_gain_hbm, gate_hbm, up_hbm, down_hbm, out_ref,
+    gate_v, up_v, down_v, route_ref, weight_ref, gain_ref, last_gain_ref, x_ref, xs, notes, note_s, tri, cols, pick, lift, pk_s, pk_r,
     part, recv_p, hid, out_o, ret_s, ret_r, comb, sum_s, sum_r, acc, sq, sq2,
-    w_sem, x_sem, own_sem, rel_sem, blk_sem, nown_sem, nrel_sem, note_sem, ks_sem, kr_sem,
+    w_sem, small_sem, x_sem, own_sem, rel_sem, blk_sem, nown_sem, nrel_sem, note_sem, ks_sem, kr_sem,
     ps_sem, pr_sem, hs_sem, hr_sem, ts_sem, tr_sem, ss_sem, sr_sem, qs_sem, qr_sem,
 ):
     me = lax.axis_index("ep")
@@ -427,7 +427,9 @@
         pltpu.make_async_copy(x_hbm.at[:, pl.ds(c * cw, cw)], x_ref.at[:, pl.ds(c * cw, cw)], x_sem.at[c])
         for c in range(parts)
     ]
-    for load in x_loads + loads:
+    small = ((route_hbm, route_ref), (weight_hbm, weight_ref), (gain_hbm, gain_ref), (last_gain_hbm, last_gain_ref))
+    small_loads = [pltpu.make_async_copy(src, dst, small_sem.at[i]) for i, (src, dst) in enumerate(small)]
+    for load in x_loads + small_loads + loads:
         load.start()
 
     barrier = pltpu.get_barrier_semaphore()
@@ -716,6 +718,8 @@
     shape = (rows_all, rows_all)
     earlier = lax.broadcasted_iota(jnp.int32, shape, 0) < lax.broadcasted_iota(jnp.int32, shape, 1)
     tri[...] = jnp.where(earlier, 1.0, 0.0).astype(BF)
+    for load in small_loads:
+        load.wait()
     blank = jnp.zeros((3, rows_all), F32)
     note_s[...] = jnp.concatenate(
         [route_ref[...].astype(F32), weight_ref[...], finish_sum(0)[0:1], blank], axis=0
@@ -790,18 +794,22 @@
     line = n // 2
     count = local * cap
     parts = 4
-    any_spec = pl.BlockSpec(memory_space=pl.ANY)
+    any_spec = pl.BlockSpec(memory_space=pltpu.HBM)
     vmem = pl.BlockSpec(memory_space=pltpu.VMEM)
     dma = pltpu.SemaphoreType.DMA
     return pl.pallas_call(
         functools.partial(line_kernel, n, nt, local, cap, full, parts),
         out_shape=jax.ShapeDtypeStruct((rows, width), BF),
-        in_specs=[any_spec, vmem, vmem, vmem, vmem, any_spec, any_spec, any_spec],
+        in_specs=[any_spec, any_spec, any_spec, any_spec, any_spec, any_spec, any_spec, any_spec],
         out_specs=vmem,
         scratch_shapes=[
             pltpu.VMEM(gate_weight.shape, BF),
             pltpu.VMEM(up_weight.shape, BF),
             pltpu.VMEM(down_weight.shape, BF),
+            pltpu.VMEM(routes.T.shape, routes.dtype),
+            pltpu.VMEM(weights.T.shape, F32),
+            pltpu.VMEM((1, width), F32),
+            pltpu.VMEM((1, width), F32),
             pltpu.VMEM((rows, width), BF),
             pltpu.VMEM((line, rows, width), BF),
             pltpu.VMEM((line, 8, rows), F32),
@@ -825,6 +833,7 @@
             pltpu.VMEM((2, 8, rows), F32),
             pltpu.VMEM((2, nt - 1, 8, rows), F32),
             dma((3,)),
+            dma((4,)),
             dma((parts,)),
             dma((2, parts)),
             dma((line - 1, parts)),

time: 147 us -> 140 us (0.952)
  Pallas kernels: 144 us -> 138 us
    pallas_call x1, Pallas kernels: 144 us -> 138 us  [line_call(): pl.pallas_call(functools.partial(line_kernel, n, nt, local, cap, full, pa...]
where the time goes in v3:
time: 140 us
  Pallas kernels  138 us (99%)
  local copies, waits for them, and re-layouts  2.26 us (2%)
    pallas_call x1, Pallas kernels, line_call(): pl.pallas_call(functools.partial(line_kernel, n, nt, local, cap, full, pa...  138 us

profile of v3, /device:TPU:9, one launch (start us, length us, event | category | flops | bytes accessed | tf_op | source)
XLA Modules:
  0.0 139.8 jit_solution(9814665931274794876)
XLA Ops:
  0.0 137.5 %shard_map.82 = bf16[512,1024]{1,0:T(8,128)(2,1)} custom-call(bf16[512,1024]{1,0:T(8,128)(2,1)} %x_hbm.1, s32[2,512]{1,0:T(2,128)} %bitcast.4, f32[2,512]{1,0:T(2,128)} %bitcast.5, f32[1,1024]{1,0:T(1,128)} %bitcast.6, f32[1,1024]{1,0:T(1,128)} %bitcast.7, bf16[2,1024,512]{2,1,0:T(8,128)(2,1)} %gate_hbm.1, bf16[2,1024,512]{2,1,0:T(8,128)(2,1)} %up_hbm.1, ...), custom_call_target="tpu_custom_call" | custom-call | tf_op jit(solution)/shard_map/pallas_call | solution.py:800
  137.5 2.3 %copy.10 = bf16[512,1024]{1,0:T(8,128)(2,1)} copy(bf16[512,1024]{1,0:T(8,128)(2,1)} %shard_map.82) | data formatting | bytes 2097152

commit v4 on v3

--- a/solution.py
+++ b/solution.py
@@ -357,42 +357,44 @@
 
 
 END_ORDER = (
-    ("prep", 1), ("a", 0, 0), ("pack", 1, 0), ("b", 0, 0), ("pack", 1, 1), ("pack", 1, 2), ("a", 0, 1), ("b",
-    0, 1), ("pack", 1, 3), ("prep", 2), ("a", 1, 0), ("a", 1, 1), ("c1", 0, 0), ("weave", 1), ("pack", 2, 0),
-    ("pack", 2, 1), ("b", 1, 0), ("b", 1, 1), ("pack", 2, 2), ("pack", 2, 3), ("a", 2, 0), ("c1", 1, 0),
-    ("c1", 1, 1), ("c1", 1, 2), ("a", 2, 1), ("c", 1), ("d", 1, 0), ("b", 2, 0), ("prep", 3), ("pack", 3, 0),
-    ("pack", 3, 1), ("weave", 2), ("d", 1, 1), ("b", 2, 1), ("d", 1, 2), ("pack", 3, 2), ("c1", 2, 0),
-    ("pack", 3, 3), ("c1", 2, 1), ("a", 3, 0), ("c", 2), ("d", 2, 0), ("c1", 2, 2), ("c1", 2, 3), ("c1", 0,
-    1), ("a", 3, 1), ("d", 2, 1), ("d", 2, 3), ("b", 3, 1), ("b", 3, 0), ("weave", 0), ("d", 2, 2), ("c1", 1,
-    3), ("weave", 3), ("c", 0), ("c1", 3, 0), ("c1", 3, 1), ("c", 3), ("d", 3, 0), ("mix0", 1), ("c1", 0, 2),
-    ("d", 3, 1), ("c1", 3, 2), ("c1", 3, 3), ("d", 3, 2), ("mix0", 0), ("c1", 0, 3), ("d", 3, 3), ("mix0", 2),
-    ("last", 0), ("mix0", 3), ("last", 3), ("d", 1, 3), ("last", 1), ("last", 2),
+    ("prep", 1), ("a", 0, 0), ("pack", 1, 0), ("pack", 1, 1), ("weave", 1), ("pack", 1, 2), ("pack", 1, 3),
+    ("a", 1, 0), ("a2", 1, 0), ("weave", 0), ("a", 0, 1), ("a", 1, 1), ("a2", 1, 1), ("b", 1, 0), ("prep", 2),
+    ("pack", 2, 0), ("pack", 2, 1), ("a2", 0, 0), ("b", 1, 1), ("weave", 2), ("a2", 0, 1), ("pack", 2, 2),
+    ("c1", 1, 0), ("pack", 2, 3), ("a", 2, 0), ("c1", 1, 1), ("c", 1), ("b", 0, 1), ("b", 0, 0), ("d", 1, 0),
+    ("c1", 1, 2), ("a", 2, 1), ("a2", 2, 1), ("d", 1, 1), ("a2", 2, 0), ("prep", 3), ("pack", 3, 0), ("b", 2,
+    1), ("d", 1, 2), ("pack", 3, 1), ("pack", 3, 2), ("b", 2, 0), ("c1", 2, 0), ("pack", 3, 3), ("a", 3, 0),
+    ("c", 2), ("d", 2, 0), ("c1", 2, 1), ("c1", 0, 0), ("c1", 2, 2), ("c1", 2, 3), ("a2", 3, 0), ("a", 3, 1),
+    ("a2", 3, 1), ("d", 2, 1), ("b", 3, 1), ("c", 0), ("c1", 0, 1), ("d", 2, 2), ("mix0", 0), ("weave", 3),
+    ("c1", 3, 0), ("c1", 3, 1), ("c1", 3, 2), ("d", 2, 3), ("b", 3, 0), ("c", 3), ("d", 3, 0), ("mix0", 1),
+    ("c1", 0, 2), ("c1", 3, 3), ("d", 3, 2), ("c1", 0, 3), ("last", 1), ("d", 3, 1), ("d", 3, 3), ("mix0", 2),
+    ("last", 2), ("c1", 1, 3), ("mix0", 3), ("last", 0), ("last", 3), ("d", 1, 3),
 )
 
 INNER_ORDER = (
-    ("a", 0, 0), ("passn", 1), ("prep", 1), ("pass", 1, 0), ("b", 0, 0), ("pass", 1, 1), ("pack", 1, 0),
-    ("pack", 1, 1), ("a", 0, 1), ("weave", 0), ("passn", 2), ("pass", 2, 0), ("pass", 1, 2), ("pack", 1, 2),
-    ("pass", 1, 3), ("c", 0), ("pack", 1, 3), ("prep", 2), ("pass", 2, 1), ("pass", 2, 2), ("a", 1, 0),
-    ("pass", 2, 3), ("ownin", 2), ("ownin", 3), ("pack", 2, 0), ("b", 0, 1), ("pack", 2, 1), ("pack", 2, 2),
-    ("a", 1, 1), ("pack", 2, 3), ("passn", 3), ("weave", 1), ("c1", 0, 0), ("prep", 3), ("pass", 3, 0), ("a",
-    2, 0), ("pass", 3, 1), ("pack", 3, 0), ("b", 1, 0), ("pass", 3, 2), ("pass", 3, 3), ("a", 2, 1), ("pack",
-    3, 1), ("pack", 3, 2), ("b", 1, 1), ("b", 2, 1), ("pack", 3, 3), ("a", 3, 0), ("c1", 0, 1), ("mix0", 1),
-    ("mix0", 0), ("c1", 2, 0), ("b", 2, 0), ("c1", 2, 1), ("c1", 2, 2), ("c1", 2, 3), ("weave", 2), ("b", 3,
-    0), ("weave", 3), ("a", 3, 1), ("c1", 1, 0), ("c", 2), ("d", 2, 0), ("b", 3, 1), ("d", 2, 1), ("c1", 1,
-    1), ("c1", 1, 2), ("c1", 1, 3), ("c", 3), ("c", 1), ("d", 1, 0), ("c1", 3, 0), ("d", 2, 3), ("d", 1, 1),
-    ("d", 2, 2), ("c1", 3, 1), ("c1", 3, 2), ("c1", 3, 3), ("c1", 0, 2), ("c1", 0, 3), ("d", 1, 3), ("d", 3,
-    0), ("d", 1, 2), ("d", 3, 1), ("d", 3, 2), ("mix0", 3), ("spare", 1), ("d", 3, 3), ("last", 1), ("spare",
-    0), ("last", 0), ("mix0", 2), ("spare", 2), ("spare", 3), ("last", 2), ("last", 3),
+    ("a", 0, 0), ("passn", 1), ("prep", 1), ("pass", 1, 0), ("passn", 3), ("a", 0, 1), ("a2", 0, 1), ("pass",
+    2, 0), ("pass", 1, 1), ("pack", 1, 0), ("pack", 1, 1), ("pass", 1, 2), ("pass", 1, 3), ("pack", 1, 2),
+    ("pack", 1, 3), ("passn", 2), ("a", 1, 0), ("a2", 1, 0), ("a2", 0, 0), ("pass", 2, 1), ("pass", 2, 2),
+    ("ownin", 2), ("b", 0, 1), ("a", 1, 1), ("a2", 1, 1), ("prep", 2), ("pack", 2, 0), ("pack", 2, 1),
+    ("pack", 2, 2), ("pass", 2, 3), ("pass", 3, 0), ("b", 1, 0), ("ownin", 3), ("pack", 2, 3), ("prep", 3),
+    ("a", 2, 0), ("pack", 3, 0), ("pass", 3, 1), ("pack", 3, 1), ("a2", 2, 0), ("b", 1, 1), ("weave", 0),
+    ("pass", 3, 2), ("b", 2, 0), ("a", 2, 1), ("a2", 2, 1), ("c", 1), ("pass", 3, 3), ("pack", 3, 2), ("pack",
+    3, 3), ("b", 2, 1), ("weave", 2), ("a", 3, 0), ("c1", 0, 0), ("c1", 0, 1), ("c", 2), ("c1", 0, 2), ("a2",
+    3, 0), ("a", 3, 1), ("c1", 0, 3), ("b", 3, 0), ("c1", 1, 0), ("c1", 2, 0), ("weave", 1), ("c1", 2, 1),
+    ("c1", 2, 2), ("c1", 1, 1), ("c1", 1, 2), ("c1", 2, 3), ("a2", 3, 1), ("c", 3), ("b", 0, 0), ("d", 2, 0),
+    ("b", 3, 1), ("d", 2, 1), ("c1", 1, 3), ("weave", 3), ("c", 0), ("mix0", 0), ("d", 1, 0), ("d", 2, 2),
+    ("mix0", 3), ("mix0", 1), ("c1", 3, 0), ("spare", 0), ("d", 1, 1), ("c1", 3, 1), ("c1", 3, 2), ("spare",
+    1), ("d", 2, 3), ("d", 1, 2), ("d", 3, 0), ("d", 1, 3), ("d", 3, 2), ("d", 3, 1), ("c1", 3, 3), ("d", 3,
+    3), ("mix0", 2), ("spare", 2), ("last", 2), ("last", 0), ("spare", 3), ("last", 1), ("last", 3),
 )
 
 
 def line_kernel(
     n, nt, local, cap, full, parts,
-    x_hbm, route_hbm, weight_hbm, gain_hbm, last_gain_hbm, gate_hbm, up_hbm, down_hbm, out_ref,
+    x_hbm, route_hbm, weight_hbm, gain_hbm, last_gain_hbm, gate_hbm, up_hbm, down_hbm, out_hbm,
     gate_v, up_v, down_v, route_ref, weight_ref, gain_ref, last_gain_ref, x_ref, xs, notes, note_s, tri, cols, pick, lift, pk_s, pk_r,
-    part, recv_p, hid, out_o, ret_s, ret_r, comb, sum_s, sum_r, acc, sq, sq2,
+    part, recv_p, pair_s, pair_r, hid, out_o, ret_s, ret_r, comb, sum_s, sum_r, acc, sq, sq2,
     w_sem, small_sem, x_sem, own_sem, rel_sem, blk_sem, nown_sem, nrel_sem, note_sem, ks_sem, kr_sem,
-    ps_sem, pr_sem, hs_sem, hr_sem, ts_sem, tr_sem, ss_sem, sr_sem, qs_sem, qr_sem,
+    ps_sem, pr_sem, ys_sem, yr_sem, hs_sem, hr_sem, ts_sem, tr_sem, ss_sem, sr_sem, qs_sem, qr_sem,
 ):
     me = lax.axis_index("ep")
     my_tp = lax.axis_index("tp")
@@ -412,6 +414,8 @@
     mate = me + 1 - 2 * side
     across = {"ep": mate, "tp": my_tp}
     spare = last + 1
+    pair, row = my_tp % 2, my_tp // 2
+    partner, facing = my_tp + 1 - 2 * pair, lax.rem(my_tp + 2, nt)
 
     def block(s):
         if s == 0:
@@ -527,11 +531,15 @@
             device_id=inward,
         ).wait_recv()
 
-    def p_copy(i, o):
-        q = lax.rem(my_tp + o, nt)
-        return pltpu.make_async_remote_copy(
-            part.at[i, q], recv_p.at[i, o - 1], ps_sem.at[i, o - 1], pr_sem.at[i, o - 1],
-            device_id={"ep": me, "tp": q},
+    def p_copy(i):
+        return pltpu.make_async_remote_copy(
+            part.at[i, pl.ds(2 * (1 - pair), 2)], recv_p.at[i], ps_sem.at[i], pr_sem.at[i],
+            device_id={"ep": me, "tp": partner},
+        )
+
+    def y_copy(i):
+        return pltpu.make_async_remote_copy(
+            pair_s.at[i], pair_r.at[i], ys_sem.at[i], yr_sem.at[i], device_id={"ep": me, "tp": facing}
         )
 
     def h_copy(i, o, back=False):
@@ -565,13 +573,16 @@
     def pack(s, c):
         values = x_ref.at[:, col(c)] if s == 0 else xs.at[block(s), :, col(c)]
 
-        @pl.loop(0, 2 * local)
-        def _(e):
-            group = pl.ds(pl.multiple_of(e * cap, cap), cap)
-            rows = dot(pick[group, :], values[...]) * lift[group, 0:1] * gain_ref[:, col(c)]
-            pk_s[s, group, col(c)] = rows.astype(BF)
-
+        def groups(first):
+            @pl.loop(first, first + local)
+            def _(e):
+                group = pl.ds(pl.multiple_of(e * cap, cap), cap)
+                rows = dot(pick[group, :], values[...]) * lift[group, 0:1] * gain_ref[:, col(c)]
+                pk_s[s, group, col(c)] = rows.astype(BF)
+
+        groups(local)
         pack_copy(s, c).start()
+        groups(0)
 
     def stage_a(s, h):
         i = 2 * s + h
@@ -587,19 +598,25 @@
             gate = dot(rows, gate_v[j]).astype(BF)
             upper = dot(rows, up_v[j]).astype(BF)
             for q in range(nt):
-                part[i, q, group, pl.ds(0, fq)] = gate[:, q * fq:(q + 1) * fq]
-                part[i, q, group, pl.ds(fq, fq)] = upper[:, q * fq:(q + 1) * fq]
-
-        for o in range(1, nt):
-            p_copy(i, o).start()
+                slab = q % 2 * 2 + q // 2
+                part[i, slab, group, pl.ds(0, fq)] = gate[:, q * fq:(q + 1) * fq]
+                part[i, slab, group, pl.ds(fq, fq)] = upper[:, q * fq:(q + 1) * fq]
+
+        p_copy(i).start()
+
+    def pair_sum(i, side_row):
+        return part[i, 2 * pair + side_row].astype(F32) + recv_p[i, side_row].astype(F32)
+
+    def stage_y(s, h):
+        i = 2 * s + h
+        p_copy(i).wait_recv()
+        pair_s[i] = pair_sum(i, 1 - row).astype(BF)
+        y_copy(i).start()
 
     def stage_b(s, h):
         i = 2 * s + h
-        for o in range(1, nt):
-            p_copy(i, o).wait_recv()
-        total = part[i, my_tp].astype(F32)
-        for o in range(1, nt):
-            total = total + recv_p[i, o - 1].astype(F32)
+        y_copy(i).wait_recv()
+        total = pair_sum(i, row) + pair_r[i].astype(F32)
         gate, upper = total[:, :fq], total[:, fq:]
         hid[i, my_tp] = (gate / (1.0 + jnp.exp(-gate)) * upper).astype(BF)
         for o in range(1, nt):
@@ -696,7 +713,7 @@
 
         calls = {
             "passn": pass_note, "pass": pass_on, "ownin": lead, "prep": prep, "pack": bring,
-            "a": stage_a, "b": stage_b, "c": stage_c, "c1": send_back, "weave": weave, "mix0": own_mix,
+            "a": stage_a, "a2": stage_y, "b": stage_b, "c": stage_c, "c1": send_back, "weave": weave, "mix0": own_mix,
             "d": lambda s, c: stage_d(s, c, not at_end), "spare": add_spare, "last": add_last,
         }
         for name, *where in order:
@@ -758,8 +775,9 @@
     send_sum(1)
 
     for i in range(2 * last + 2):
-        for o in range(1, nt):
-            p_copy(i, o).wait_send()
+        p_copy(i).wait_send()
+        y_copy(i).wait_send()
+        for o in range(1, nt):
             h_copy(i, o).wait_send()
     for s in range(last + 1):
         for c in range(parts):
@@ -782,7 +800,15 @@
                 relay(s, c).wait_send()
 
     scale = jnp.sum(jnp.where(eye(), finish_sum(1)[0:1], 0.0), axis=1, keepdims=True)
-    out_ref[...] = (acc[...] * scale * last_gain_ref[...]).astype(BF)
+    rows_k = rows_all // parts
+    stores = []
+    for k in range(parts):
+        band = pl.ds(k * rows_k, rows_k)
+        x_ref[band, :] = (acc[band, :] * scale[k * rows_k:(k + 1) * rows_k] * last_gain_ref[...]).astype(BF)
+        stores.append(pltpu.make_async_copy(x_ref.at[band, :], out_hbm.at[band, :], x_sem.at[k]))
+        stores[-1].start()
+    for store in stores:
+        store.wait()
     for k in range(2):
         for o in range(1, nt):
             sq_copy(k, o).wait_send()
@@ -795,13 +821,12 @@
     count = local * cap
     parts = 4
     any_spec = pl.BlockSpec(memory_space=pltpu.HBM)
-    vmem = pl.BlockSpec(memory_space=pltpu.VMEM)
     dma = pltpu.SemaphoreType.DMA
     return pl.pallas_call(
         functools.partial(line_kernel, n, nt, local, cap, full, parts),
         out_shape=jax.ShapeDtypeStruct((rows, width), BF),
         in_specs=[any_spec, any_spec, any_spec, any_spec, any_spec, any_spec, any_spec, any_spec],
-        out_specs=vmem,
+        out_specs=any_spec,
         scratch_shapes=[
             pltpu.VMEM(gate_weight.shape, BF),
             pltpu.VMEM(up_weight.shape, BF),
@@ -821,7 +846,9 @@
             pltpu.VMEM((line, 2 * count, width), BF),
             pltpu.VMEM((line, count, width), BF),
             pltpu.VMEM((n, nt, count, 2 * ff // nt), BF),
-            pltpu.VMEM((n, nt - 1, count, 2 * ff // nt), BF),
+            pltpu.VMEM((n, 2, count, 2 * ff // nt), BF),
+            pltpu.VMEM((n, count, 2 * ff // nt), BF),
+            pltpu.VMEM((n, count, 2 * ff // nt), BF),
             pltpu.VMEM((n, nt, count, ff // nt), BF),
             pltpu.VMEM((line, count, width), BF),
             pltpu.VMEM((line, count, width), BF),
@@ -843,10 +870,12 @@
             dma((line,)),
             dma((line, parts)),
             dma((line, parts)),
-            dma((n, nt - 1)),
-            dma((n, nt - 1)),
-            dma((n, nt - 1)),
-            dma((n, nt - 1)),
+            dma((n,)),
+            dma((n,)),
+            dma((n,)),
+            dma((n,)),
+            dma((n, 3)),
+            dma((n, 3)),
             dma((line, parts)),
             dma((line, parts)),
             dma((line - 1, parts)),
@@ -873,7 +902,7 @@
     count = local * cap
     blocks = max(n - 4, 0)
     ring = n % 2 == 0 and n >= 6 and local % 2 == 0 and blocks * rows * width * 2 <= RING_BYTES
-    if n == 8 and local <= 8 and width % 512 == 0 and cap % 128 == 0:
+    if n == 8 and nt == 4 and local <= 8 and width % 512 == 0 and cap % 128 == 0:
         return line_call(
             n, nt, local, cap, full, tokens, routes, route_weights, norm_gain, gate_weight, up_weight, down_weight, final_gain
         )

time: 140 us -> 139 us (level)
  Pallas kernels: 138 us -> 136 us
where the time goes in v4:
time: 139 us
  Pallas kernels  136 us (98%)
  local copies, waits for them, and re-layouts  2.26 us (2%)
    pallas_call x1, Pallas kernels, line_call(): pl.pallas_call(functools.partial(line_kernel, n, nt, local, cap, full, pa...  136 us

profile of v4, /device:TPU:9, one launch (start us, length us, event | category | flops | bytes accessed | tf_op | source)
XLA Modules:
  0.0 138.6 jit_solution(17847118864432843685)
XLA Ops:
  0.0 136.3 %shard_map.82 = bf16[512,1024]{1,0:T(8,128)(2,1)} custom-call(bf16[512,1024]{1,0:T(8,128)(2,1)} %x_hbm.1, s32[2,512]{1,0:T(2,128)} %bitcast.4, f32[2,512]{1,0:T(2,128)} %bitcast.5, f32[1,1024]{1,0:T(1,128)} %bitcast.6, f32[1,1024]{1,0:T(1,128)} %bitcast.7, bf16[2,1024,512]{2,1,0:T(8,128)(2,1)} %gate_hbm.1, bf16[2,1024,512]{2,1,0:T(8,128)(2,1)} %up_hbm.1, ...), custom_call_target="tpu_custom_call" | custom-call | tf_op jit(solution)/shard_map/pallas_call | solution.py:825
  136.3 2.3 %copy.10 = bf16[512,1024]{1,0:T(8,128)(2,1)} copy(bf16[512,1024]{1,0:T(8,128)(2,1)} %shard_map.82) | data formatting | bytes 2097152
